TPU v7x, 32 devices: a whole 2x2x4 slice. The times are simulated.
32 devices in a mesh: ra: 4 (over z), cb: 4 (over y, x), dp: 2 (over core).
Axes of the slice: x: 2, y: 2, z: 4, core: 2. Of those that a mesh axis runs over, the one named last changes fastest.
Arguments:
- tokens: bfloat16 [2, 512, 4096], P('dp', None, 'ra'), may hold values from -80 to 80
- pre_gain: float32 [4096], P('ra'), may hold values from 0.1 to 1.9
- w_gate: bfloat16 [4096, 11264], P('ra', 'cb'), may hold values from -0.09375 to 0.09375
- w_up: bfloat16 [4096, 11264], P('ra', 'cb'), may hold values from -0.09375 to 0.09375
- conv_gate: float32 [3, 11264], P(None, 'cb'), may hold values from -3.5 to 3.5
- conv_up: float32 [3, 11264], P(None, 'cb'), may hold values from -3.5 to 3.5
- w_down: bfloat16 [11264, 4096], P('cb', 'ra'), may hold values from -2 to 2
- post_gain: float32 [4096], P('ra'), may hold values from 0.1 to 1.9
Outputs:
- mixed: bfloat16 [2, 512, 4096], P('dp', None, 'ra')
All inputs are finite; a program needn't handle non-finite values.
Results may differ from a plain program's by a relative error of at most 0.0064.
Values may be sent and summed in bfloat16 or wider, within the bound.
A program may use at most 128 MiB of HBM per device.

v0:
```python
import functools
import jax
import jax.numpy as jnp
from jax import lax
from jax.experimental import pallas as pl
from jax.experimental.pallas import tpu as pltpu
from jax.sharding import PartitionSpec as P

epsilon = 1e-06
residual_scale = 0.125
LANES = 128
HALO = 16
MESH = pl.DeviceIdType.MESH


def gelu(v):
    return 0.5 * v * (1.0 + jnp.tanh(0.7978845608028654 * (v + 0.044715 * v * v * v)))


def kernel(
    n, m, wire,
    tok_ref, pre_ref, wg_hbm, wu_hbm, cg_ref, cu_ref, wd_hbm, post_ref, out_ref,
    wg, wu, wd, xw, gu, rbuf, sbuf, hid, acc, sq_out, sq_in, scale, bsend, brecv, ps_out, ps_in,
    wsem, dsem, psend, precv, hsend, hrecv, sqs, sqr, bss, bsr, pss, psr, oss, osr,
):
    rows, width = tok_ref.shape
    chunks = rbuf.shape[1] // 2
    part = rows // 2
    span = part + HALO
    half = chunks * LANES
    block = part // m
    dim_full = width * n
    r = lax.axis_index("ra")
    me = lax.axis_index("cb")
    f32, bf16 = jnp.float32, jnp.bfloat16

    def units(d, c):
        return pl.ds(pl.multiple_of(d * half + c * LANES, LANES), LANES)

    def weight_copies(d, c):
        at = units(d, c)
        return (
            pltpu.make_async_copy(wg_hbm.at[:, at], wg.at[:, at], wsem.at[0, d, c]),
            pltpu.make_async_copy(wu_hbm.at[:, at], wu.at[:, at], wsem.at[1, d, c]),
        )

    first = (2 * r) // n

    def fetch(c, carry):
        for i in (0, 1):
            for copy in weight_copies((i + first) % 2, c):
                copy.start()
        return carry

    lax.fori_loop(0, chunks, fetch, 0)
    down_copy = pltpu.make_async_copy(wd_hbm, wd, dsem)
    down_copy.start()

    barrier = pltpu.get_barrier_semaphore()
    for k in range(1, n):
        pl.semaphore_signal(barrier, inc=1, device_id={"ra": (r + k) % n}, device_id_type=MESH)
    for k in range(1, m):
        pl.semaphore_signal(barrier, inc=1, device_id={"cb": (me + k) % m}, device_id_type=MESH)

    values = tok_ref[...].astype(f32)
    xw[...] = (values * pre_ref[...]).astype(bf16)
    square = values * values
    high = square.astype(bf16)
    low = (square - high.astype(f32)).astype(bf16)
    ones = jnp.ones((8, width), bf16)
    nt = (((1,), (1,)), ((), ()))
    sq_out[...] = lax.dot_general(ones, high, nt, preferred_element_type=f32) + lax.dot_general(
        ones, low, nt, preferred_element_type=f32
    )
    acc[...] = jnp.zeros_like(acc)
    pl.semaphore_wait(barrier, n - 1 + m - 1)

    def square_copy(end, k):
        return pltpu.make_async_remote_copy(
            src_ref=sq_out, dst_ref=sq_in.at[k],
            send_sem=sqs.at[end], recv_sem=sqr.at[k],
            device_id={"ra": end * (n - 1)}, device_id_type=MESH,
        )

    for end in (0, 1):
        @pl.when(r != end * (n - 1))
        def _():
            square_copy(end, r).start()

    def partial_copy(d, c):
        return pltpu.make_async_remote_copy(
            src_ref=sbuf.at[d, c], dst_ref=rbuf.at[d, c],
            send_sem=psend.at[d, c], recv_sem=precv.at[d, c],
            device_id={"ra": (r + 1 - 2 * d + n) % n}, device_id_type=MESH,
        )

    def hidden_copy(d, c):
        return pltpu.make_async_remote_copy(
            src_ref=hid.at[d, c, kept(c // chunks)], dst_ref=hid.at[d, c, kept(c // chunks)],
            send_sem=hsend.at[d, c], recv_sem=hrecv.at[d, c],
            device_id={"ra": (r - 1 + 2 * d + n) % n}, device_id_type=MESH,
        )

    def place(d):
        return r * (1 - d) + (n - 1 - r) * d

    def total_scale():
        total = sq_out[...]
        for k in range(n):
            @pl.when(r != k)
            def _():
                square_copy(0, k).wait_recv()
            total = total + jnp.where(r != k, sq_in[k], 0.0)
        inv = lax.rsqrt(total / dim_full + epsilon)
        scale[...] = jnp.concatenate([inv] * (LANES // 8), axis=0).T

    def taken(q):
        return pl.ds(pl.multiple_of(q * (part - HALO), HALO), span)

    def kept(q):
        return pl.ds(pl.multiple_of(q * HALO, HALO), part)

    def convolve(field, taps_ref, at, q):
        spot = lax.broadcasted_iota(jnp.int32, field.shape, 0) + q * (part - HALO)
        before = jnp.where(spot == 0, 0.0, pltpu.roll(field, 1, 0))
        after = jnp.where(spot == rows - 1, 0.0, pltpu.roll(field, span - 1, 0))
        return taps_ref[0:1, at] * before + taps_ref[1:2, at] * field + taps_ref[2:3, at] * after

    def step(s, carry):
        for i in (0, 1):
            d = (i + first) % 2
            p = place(d)
            c = s - p

            @pl.when((c >= 0) & (c < 2 * chunks))
            def _():
                q = c // chunks
                u = c % chunks
                at = units(d, u)

                @pl.when(q == 0)
                def _():
                    for copy in weight_copies(d, u):
                        copy.wait()

                gu[:, :LANES] = jnp.dot(xw[taken(q), :], wg[:, at], preferred_element_type=f32)
                gu[:, LANES:] = jnp.dot(xw[taken(q), :], wu[:, at], preferred_element_type=f32)

                @pl.when(p == 0)
                def _():
                    sbuf[d, c] = gu[...].astype(wire)
                    partial_copy(d, c).start()

                @pl.when(p > 0)
                def _():
                    partial_copy(d, c).wait_recv()

                @pl.when((p > 0) & (p < n - 1))
                def _():
                    sbuf[d, c] = (gu[...] + rbuf[d, c].astype(f32)).astype(wire)
                    partial_copy(d, c).start()

                @pl.when(p == n - 1)
                def _():
                    @pl.when(c == 0)
                    def _():
                        total_scale()

                    by = scale[taken(q), :]
                    gate_lin = (gu[:, :LANES] + rbuf[d, c, :, :LANES].astype(f32)) * by
                    up_lin = (gu[:, LANES:] + rbuf[d, c, :, LANES:].astype(f32)) * by
                    gate_conv = convolve(gate_lin, cg_ref, at, q)
                    up_conv = convolve(up_lin, cu_ref, at, q)
                    hid[d, c] = (gelu(gate_conv) * up_conv).astype(bf16)
                    hidden_copy(d, c).start()

        @pl.when(s == n - 1)
        def _():
            down_copy.wait()

        for i in (0, 1):
            d = (1 - i + first) % 2
            p = place(d)
            c = s - 2 * (n - 1) + p

            @pl.when((c >= 0) & (c < 2 * chunks))
            def _():
                q = c // chunks

                @pl.when(p < n - 1)
                def _():
                    hidden_copy(d, c).wait_recv()

                @pl.when((p > 0) & (p < n - 1))
                def _():
                    hidden_copy(d, c).start()

                at = pl.ds(pl.multiple_of(q * part, part), part)
                acc[at, :] += jnp.dot(
                    hid[d, c, kept(q), :], wd[units(d, c % chunks), :], preferred_element_type=f32
                )

        @pl.when(s == first_done)
        def _():
            send_branch(0)

        @pl.when(s == first_done + chunks // 3)
        def _():
            sum_branch(0)

        @pl.when(s == first_done + 2 * chunks // 3)
        def _():
            send_mixed(0)

        return carry

    first_done = chunks - 1 + 2 * (n - 1)

    def rows_of(q, j):
        return pl.ds(pl.multiple_of(q * part + j * block, block), block)

    def branch_copy(q, k):
        peer = (me + k) % m
        return pltpu.make_async_remote_copy(
            src_ref=bsend.at[rows_of(q, peer)], dst_ref=brecv.at[q, k],
            send_sem=bss.at[q, k], recv_sem=bsr.at[q, k],
            device_id={"cb": peer}, device_id_type=MESH,
        )

    def post_copy(q, k):
        return pltpu.make_async_remote_copy(
            src_ref=ps_out.at[q], dst_ref=ps_in.at[q, k],
            send_sem=pss.at[q, k], recv_sem=psr.at[q, k],
            device_id={"ra": (r + k) % n}, device_id_type=MESH,
        )

    def out_copy(q, k):
        mine = rows_of(q, me)
        return pltpu.make_async_remote_copy(
            src_ref=out_ref.at[mine], dst_ref=out_ref.at[mine],
            send_sem=oss.at[q, k], recv_sem=osr.at[q, k],
            device_id={"cb": (me + k) % m}, device_id_type=MESH,
        )

    def send_branch(q):
        at = pl.ds(q * part, part)
        bsend[at, :] = acc[at, :].astype(wire)
        for k in range(1, m):
            branch_copy(q, k).start()

    def sum_branch(q):
        mine = rows_of(q, me)
        branch = acc[mine, :]
        for k in range(1, m):
            branch_copy(q, k).wait_recv()
            branch = branch + brecv[q, k].astype(f32)
        acc[mine, :] = branch
        ps_out[q] = jnp.broadcast_to(jnp.sum(branch * branch, axis=1, keepdims=True), (block, LANES))
        for k in range(1, n):
            post_copy(q, k).start()

    def send_mixed(q):
        mine = rows_of(q, me)
        total = ps_out[q]
        for k in range(1, n):
            post_copy(q, k).wait_recv()
            total = total + ps_in[q, k]
        inv = lax.rsqrt(total[:, 0:1] / dim_full + epsilon)
        mixed = residual_scale * tok_ref[mine, :].astype(f32) + acc[mine, :] * inv * post_ref[...]
        out_ref[mine, :] = mixed.astype(bf16)
        for k in range(1, m):
            out_copy(q, k).start()

    lax.fori_loop(0, 2 * chunks + 2 * (n - 1), step, 0)
    send_branch(1)

    for end in (0, 1):
        @pl.when(r != end * (n - 1))
        def _():
            square_copy(end, r).wait_send()

    def drain(c, carry):
        for d in (0, 1):
            p = place(d)

            @pl.when(p < n - 1)
            def _():
                partial_copy(d, c).wait_send()

            @pl.when(p > 0)
            def _():
                hidden_copy(d, c).wait_send()
        return carry

    lax.fori_loop(0, 2 * chunks, drain, 0)
    sum_branch(1)
    send_mixed(1)
    for q in (0, 1):
        for k in range(1, m):
            branch_copy(q, k).wait_send()
            out_copy(q, k).wait()
        for k in range(1, n):
            post_copy(q, k).wait_send()


def local(n, m, tokens, pre_gain, w_gate, w_up, conv_gate, conv_up, w_down, post_gain):
    rows, width = tokens.shape[1:]
    total_units = w_gate.shape[1]
    chunks = total_units // (2 * LANES)
    block = rows // (2 * m)
    span = rows // 2 + HALO
    wire = jnp.bfloat16 if n <= 4 else jnp.float32
    f32, bf16 = jnp.float32, jnp.bfloat16
    vmem = pl.BlockSpec(memory_space=pltpu.VMEM)
    hbm = pl.BlockSpec(memory_space=pl.ANY)
    dma = pltpu.SemaphoreType.DMA
    out = pl.pallas_call(
        functools.partial(kernel, n, m, wire),
        out_shape=jax.ShapeDtypeStruct((rows, width), bf16),
        in_specs=[vmem, vmem, hbm, hbm, vmem, vmem, hbm, vmem],
        out_specs=vmem,
        scratch_shapes=[
            pltpu.VMEM(w_gate.shape, bf16),
            pltpu.VMEM(w_up.shape, bf16),
            pltpu.VMEM(w_down.shape, bf16),
            pltpu.VMEM((rows, width), bf16),
            pltpu.VMEM((span, 2 * LANES), f32),
            pltpu.VMEM((2, 2 * chunks, span, 2 * LANES), wire),
            pltpu.VMEM((2, 2 * chunks, span, 2 * LANES), wire),
            pltpu.VMEM((2, 2 * chunks, span, LANES), bf16),
            pltpu.VMEM((rows, width), f32),
            pltpu.VMEM((8, rows), f32),
            pltpu.VMEM((n, 8, rows), f32),
            pltpu.VMEM((rows, LANES), f32),
            pltpu.VMEM((rows, width), wire),
            pltpu.VMEM((2, m, block, width), wire),
            pltpu.VMEM((2, block, LANES), f32),
            pltpu.VMEM((2, n, block, LANES), f32),
            dma((2, 2, chunks)), dma,
            dma((2, 2 * chunks)), dma((2, 2 * chunks)), dma((2, 2 * chunks)), dma((2, 2 * chunks)),
            dma((2,)), dma((n,)), dma((2, m)), dma((2, m)), dma((2, n)), dma((2, n)), dma((2, m)), dma((2, m)),
        ],
        compiler_params=pltpu.CompilerParams(
            collective_id=0, has_side_effects=True, vmem_limit_bytes=60 * 1024 * 1024
        ),
    )(tokens[0], pre_gain[None], w_gate, w_up, conv_gate, conv_up, w_down, post_gain[None])
    return out[None]


def solution(mesh):
    in_specs = (
        P("dp", None, "ra"),
        P("ra"),
        P("ra", "cb"),
        P("ra", "cb"),
        P(None, "cb"),
        P(None, "cb"),
        P("cb", "ra"),
        P("ra"),
    )
    out_specs = P("dp", None, "ra")
    return jax.shard_map(
        functools.partial(local, mesh.shape["ra"], mesh.shape["cb"]),
        mesh=mesh, in_specs=in_specs, out_specs=out_specs, check_vma=False,
    )
```

profile of v0, /device:TPU:0, one launch (start us, length us, event | category | flops | bytes accessed | tf_op | source)
XLA Modules:
  0.0 149.5 jit_solution(17569617026973839269)
XLA Ops:
  0.0 147.2 %shard_map.82 = bf16[512,1024]{1,0:T(8,128)(2,1)} custom-call(bf16[512,1024]{1,0:T(8,128)(2,1)} %bitcast.5, f32[1,1024]{1,0:T(1,128)} %bitcast.6, bf16[1024,2816]{1,0:T(8,128)(2,1)} %wg_hbm.1, bf16[1024,2816]{1,0:T(8,128)(2,1)} %wu_hbm.1, f32[3,2816]{1,0:T(4,128)} %cg_ref.1, f32[3,2816]{1,0:T(4,128)} %cu_ref.1, bf16[2816,1024]{1,0:T(8,128)(2,1)} %wd_hbm.1, ...), custom_call_target="tpu_custom_call" | custom-call | tf_op jit(solution)/shard_map/pallas_call | solution.py:317
  147.2 2.3 %copy.10 = bf16[1,512,1024]{2,1,0:T(8,128)(2,1)} copy(bf16[1,512,1024]{2,1,0:T(8,128)(2,1)} %bitcast.4) | data formatting | bytes 2097152
where the time goes:
time: 150 us; the launch traced here: 149 us
  Pallas kernels  147 us (98%)
  local copies, waits for them, and re-layouts  2.26 us (2%)
    pallas_call x1, Pallas kernels, local(): pl.pallas_call(functools.partial(kernel, n, m, wire), out_shape=jax.Shape...  147 us

commit v1 on v0

v1 whole, which is shorter than its diff:
```python
import functools
import jax
import jax.numpy as jnp
from jax import lax
from jax.experimental import pallas as pl
from jax.experimental.pallas import tpu as pltpu
from jax.sharding import PartitionSpec as P

epsilon = 1e-06
residual_scale = 0.125
LANES = 128
PART = 128
BLOCK = 64
LAG = 4
MESH = pl.DeviceIdType.MESH


def gelu(v):
    return 0.5 * v * (1.0 + jnp.tanh(0.7978845608028654 * (v + 0.044715 * v * v * v)))


class Plan:
    def __init__(self, n, m, rows, chunks):
        self.parts = rows // PART
        self.blocks = rows // BLOCK
        self.partials = chunks * self.parts
        self.early = (chunks * 5) // 11
        reach = LAG * (n - 1)
        self.a = max(self.partials, self.early * self.parts + reach)
        self.b = max(self.a + self.blocks, self.partials + reach)
        self.end = self.b + self.blocks
        self.sum_after = 2
        self.mix_at = self.b + reach + self.sum_after + 2
        self.slots = self.mix_at + self.blocks


def kernel(
    n, m, plan,
    tok_hbm, pre_hbm, wg_hbm, wu_hbm, cg_hbm, cu_hbm, wd_hbm, post_hbm, out_ref,
    tok, pre, cg, cu, post,
    w, wd, xw, rbuf, sbuf, full, hid_a, hid_b, acc, sq_out, sq_in, scale, bsend, brecv, ps_out, ps_in,
    lsem, wsem, dsem, psend, precv, hsend, hrecv, sqs, sqr, bss, bsr, pss, psr, oss, osr,
):
    rows, width = tok.shape
    wire = sbuf.dtype
    chunks = w.shape[1]
    half = chunks * LANES
    parts, blocks = plan.parts, plan.blocks
    early = plan.early
    own_rows = BLOCK // m
    dim_full = width * n
    r = lax.axis_index("ra")
    me = lax.axis_index("cb")
    f32, bf16 = jnp.float32, jnp.bfloat16

    def weight_copies(d, c):
        at = pl.ds(pl.multiple_of(d * half + c * LANES, LANES), LANES)
        return (
            pltpu.make_async_copy(wg_hbm.at[:, at], w.at[d, c, :, pl.ds(0, LANES)], wsem.at[0, d, c]),
            pltpu.make_async_copy(wu_hbm.at[:, at], w.at[d, c, :, pl.ds(LANES, LANES)], wsem.at[1, d, c]),
        )

    tok_copies = [
        pltpu.make_async_copy(tok_hbm.at[pl.ds(q * PART, PART)], tok.at[pl.ds(q * PART, PART)], lsem.at[q])
        for q in range(parts)
    ]
    pre_copy = pltpu.make_async_copy(pre_hbm, pre, lsem.at[parts])
    rest = [
        pltpu.make_async_copy(cg_hbm, cg, lsem.at[parts + 1]),
        pltpu.make_async_copy(cu_hbm, cu, lsem.at[parts + 2]),
        pltpu.make_async_copy(post_hbm, post, lsem.at[parts + 3]),
    ]
    pre_copy.start()
    tok_copies[0].start()
    for d in (0, 1):
        for copy in weight_copies(d, 0):
            copy.start()

    barrier = pltpu.get_barrier_semaphore()
    for k in range(1, n):
        pl.semaphore_signal(barrier, inc=1, device_id={"ra": (r + k) % n}, device_id_type=MESH)
    for k in range(1, m):
        pl.semaphore_signal(barrier, inc=1, device_id={"cb": (me + k) % m}, device_id_type=MESH)

    for copy in tok_copies[1:]:
        copy.start()
    for copy in rest:
        copy.start()

    def fetch(c, carry):
        for d in (0, 1):
            for copy in weight_copies(d, c):
                copy.start()
        return carry

    lax.fori_loop(1, chunks, fetch, 0)
    down_copy = pltpu.make_async_copy(wd_hbm, wd, dsem)
    down_copy.start()

    full[pl.ds(0, 8), :] = jnp.zeros((8, 2 * LANES), f32)
    full[pl.ds(rows + 8, 8), :] = jnp.zeros((8, 2 * LANES), f32)

    def square_copy(end, k):
        return pltpu.make_async_remote_copy(
            src_ref=sq_out, dst_ref=sq_in.at[k],
            send_sem=sqs.at[end], recv_sem=sqr.at[k],
            device_id={"ra": end * (n - 1)}, device_id_type=MESH,
        )

    def send_squares():
        values = tok[...].astype(f32)
        square = values * values
        high = square.astype(bf16)
        low = (square - high.astype(f32)).astype(bf16)
        ones = jnp.ones((8, width), bf16)
        nt = (((1,), (1,)), ((), ()))
        sq_out[...] = lax.dot_general(ones, high, nt, preferred_element_type=f32) + lax.dot_general(
            ones, low, nt, preferred_element_type=f32
        )
        for end in (0, 1):
            @pl.when(r != end * (n - 1))
            def _():
                square_copy(end, r).start()

    def total_scale():
        total = sq_out[...]
        for k in range(n):
            @pl.when(r != k)
            def _():
                square_copy(0, k).wait_recv()
            total = total + jnp.where(r != k, sq_in[k], 0.0)
        inv = lax.rsqrt(total / dim_full + epsilon)
        scale[...] = jnp.concatenate([inv] * (LANES // 8), axis=0).T

    def place(d):
        return r * (1 - d) + (n - 1 - r) * d

    def part_rows(b):
        return pl.ds(pl.multiple_of(b * PART, PART), PART)

    def block_rows(b):
        return pl.ds(pl.multiple_of(b * BLOCK, BLOCK), BLOCK)

    def onward(d):
        return {"ra": (r + 1 - 2 * d + n) % n}

    def partial_copy(d, c, b):
        at = part_rows(b)
        return pltpu.make_async_remote_copy(
            src_ref=sbuf.at[d, c, at], dst_ref=rbuf.at[d, c, at],
            send_sem=psend.at[d, c, b], recv_sem=precv.at[d, c, b],
            device_id=onward(d), device_id_type=MESH,
        )

    def hidden_copy(d, g, b):
        hid = (hid_a, hid_b)[g]
        at = block_rows(b)
        return pltpu.make_async_remote_copy(
            src_ref=hid.at[1 - d, at], dst_ref=hid.at[1 - d, at],
            send_sem=hsend.at[d, g, b], recv_sem=hrecv.at[d, g, b],
            device_id=onward(d), device_id_type=MESH,
        )

    def finish_chunk(d, c):
        at = pl.ds(pl.multiple_of(d * half + c * LANES, LANES), LANES)
        taps_g, taps_u = cg[:, at], cu[:, at]
        for j in range(rows // BLOCK):
            window = full[pl.ds(j * BLOCK, BLOCK + 16), :]
            before = pltpu.roll(window, 1, 0)[8:8 + BLOCK]
            here = window[8:8 + BLOCK]
            after = pltpu.roll(window, BLOCK + 15, 0)[8:8 + BLOCK]
            conv = []
            for side, taps in ((0, taps_g), (1, taps_u)):
                lanes = slice(side * LANES, (side + 1) * LANES)
                conv.append(
                    taps[0:1] * before[:, lanes] + taps[1:2] * here[:, lanes] + taps[2:3] * after[:, lanes]
                )
            value = (gelu(conv[0]) * conv[1]).astype(bf16)

            @pl.when(c < early)
            def _():
                hid_a[d, pl.ds(j * BLOCK, BLOCK), pl.ds(pl.multiple_of(jnp.minimum(c, early - 1) * LANES, LANES), LANES)] = value

            @pl.when(c >= early)
            def _():
                hid_b[d, pl.ds(j * BLOCK, BLOCK), pl.ds(pl.multiple_of(jnp.maximum(c - early, 0) * LANES, LANES), LANES)] = value

    def partial_step(d, i):
        p = place(d)
        c = i // parts
        b = i % parts
        at = part_rows(b)

        @pl.when(b == 0)
        def _():
            for copy in weight_copies(d, c):
                copy.wait()

        own = jnp.dot(xw[at, :], w[d, c], preferred_element_type=f32)

        @pl.when(p == 0)
        def _():
            sbuf[d, c, at] = own.astype(wire)
            partial_copy(d, c, b).start()

        @pl.when((p > 0) & (p < n - 1))
        def _():
            partial_copy(d, c, b).wait_recv()
            sbuf[d, c, at] = (own + rbuf[d, c, at].astype(f32)).astype(wire)
            partial_copy(d, c, b).start()

        @pl.when(p == n - 1)
        def _():
            @pl.when(i == 0)
            def _():
                total_scale()

            partial_copy(d, c, b).wait_recv()
            by = scale[at, :]
            total = own + rbuf[d, c, at].astype(f32)
            to = pl.ds(pl.multiple_of(b * PART + 8, 8), PART)
            full[to, :LANES] = total[:, :LANES] * by
            full[to, LANES:] = total[:, LANES:] * by

            @pl.when(b == parts - 1)
            def _():
                finish_chunk(d, c)

    def hidden_step(d, g, b):
        p = place(d)
        hid = (hid_a, hid_b)[g]

        @pl.when(p > 0)
        def _():
            hidden_copy(d, g, b).wait_recv()

        @pl.when(p < n - 1)
        def _():
            hidden_copy(d, g, b).start()

        at = block_rows(b)
        first = (1 - d) * half + g * early * LANES
        deep = hid.shape[2]
        acc[at, :] += jnp.dot(hid[1 - d, at, :], wd[pl.ds(first, deep), :], preferred_element_type=f32)

    def mine(b):
        return pl.ds(pl.multiple_of(b * BLOCK + me * own_rows, own_rows), own_rows)

    def branch_copy(b, k):
        peer = (me + k) % m
        at = pl.ds(pl.multiple_of(b * BLOCK + peer * own_rows, own_rows), own_rows)
        return pltpu.make_async_remote_copy(
            src_ref=bsend.at[at], dst_ref=brecv.at[b, k],
            send_sem=bss.at[b, k], recv_sem=bsr.at[b, k],
            device_id={"cb": peer}, device_id_type=MESH,
        )

    def post_copy(b, k):
        return pltpu.make_async_remote_copy(
            src_ref=ps_out.at[b], dst_ref=ps_in.at[b, k],
            send_sem=pss.at[b, k], recv_sem=psr.at[b, k],
            device_id={"ra": (r + k) % n}, device_id_type=MESH,
        )

    def out_copy(b, k):
        return pltpu.make_async_remote_copy(
            src_ref=out_ref.at[mine(b)], dst_ref=out_ref.at[mine(b)],
            send_sem=oss.at[b, k], recv_sem=osr.at[b, k],
            device_id={"cb": (me + k) % m}, device_id_type=MESH,
        )

    def send_branch(b):
        at = block_rows(b)
        bsend[at, :] = acc[at, :].astype(wire)
        for k in range(1, m):
            branch_copy(b, k).start()

    def sum_branch(b):
        branch = acc[mine(b), :]
        for k in range(1, m):
            branch_copy(b, k).wait_recv()
            branch = branch + brecv[b, k].astype(f32)
        acc[mine(b), :] = branch
        ps_out[b] = jnp.broadcast_to(jnp.sum(branch * branch, axis=1, keepdims=True), (own_rows, LANES))
        for k in range(1, n):
            post_copy(b, k).start()

    def send_mixed(b):
        total = ps_out[b]
        for k in range(1, n):
            post_copy(b, k).wait_recv()
            total = total + ps_in[b, k]
        inv = lax.rsqrt(total[:, 0:1] / dim_full + epsilon)
        at = mine(b)
        mixed = residual_scale * tok[at, :].astype(f32) + acc[at, :] * inv * post[...]
        out_ref[at, :] = mixed.astype(bf16)
        for k in range(1, m):
            out_copy(b, k).start()

    pre_copy.wait()

    def slot(s, carry):
        @pl.when(s < parts)
        def _():
            q = jnp.minimum(s, parts - 1)
            at = part_rows(q)
            pltpu.make_async_copy(tok_hbm.at[at], tok.at[at], lsem.at[q]).wait()
            xw[at, :] = (tok[at, :].astype(f32) * pre[...]).astype(bf16)

        @pl.when(s == 0)
        def _():
            pl.semaphore_wait(barrier, n - 1 + m - 1)

        @pl.when(s == parts)
        def _():
            for copy in rest:
                copy.wait()
            send_squares()
            acc[...] = jnp.zeros_like(acc)

        @pl.when(s == plan.a)
        def _():
            down_copy.wait()

        for d in (0, 1):
            i = s - LAG * place(d)

            @pl.when((i >= 0) & (i < plan.partials))
            def _():
                partial_step(d, i)

        for d in (0, 1):
            i = s - LAG * place(d)
            for g, first in ((0, plan.a), (1, plan.b)):
                @pl.when((i >= first) & (i < first + blocks))
                def _():
                    hidden_step(d, g, i - first)

        send_at = s - plan.b - LAG * jnp.maximum(r, n - 1 - r)

        @pl.when((send_at >= 0) & (send_at < blocks))
        def _():
            send_branch(send_at)

        sum_at = send_at - plan.sum_after

        @pl.when((sum_at >= 0) & (sum_at < blocks))
        def _():
            sum_branch(sum_at)

        mix_at = s - plan.mix_at

        @pl.when(mix_at >= 0)
        def _():
            send_mixed(mix_at)

        return carry

    lax.fori_loop(0, plan.slots, slot, 0)

    for end in (0, 1):
        @pl.when(r != end * (n - 1))
        def _():
            square_copy(end, r).wait_send()

    for d in (0, 1):
        @pl.when(place(d) < n - 1)
        def _():
            def drain_partials(i, carry):
                partial_copy(d, i // parts, i % parts).wait_send()
                return carry

            def drain_hidden(b, carry):
                for g in (0, 1):
                    hidden_copy(d, g, b).wait_send()
                return carry

            lax.fori_loop(0, plan.partials, drain_partials, 0)
            lax.fori_loop(0, blocks, drain_hidden, 0)

    def drain(b, carry):
        for k in range(1, m):
            branch_copy(b, k).wait_send()
            out_copy(b, k).wait()
        for k in range(1, n):
            post_copy(b, k).wait_send()
        return carry

    lax.fori_loop(0, blocks, drain, 0)


def local(n, m, tokens, pre_gain, w_gate, w_up, conv_gate, conv_up, w_down, post_gain):
    rows, width = tokens.shape[1:]
    chunks = w_gate.shape[1] // (2 * LANES)
    half = chunks * LANES
    plan = Plan(n, m, rows, chunks)
    parts, blocks = plan.parts, plan.blocks
    own_rows = BLOCK // m
    wire = jnp.bfloat16 if n <= 4 else jnp.float32
    f32, bf16 = jnp.float32, jnp.bfloat16
    hbm = pl.BlockSpec(memory_space=pl.ANY)
    dma = pltpu.SemaphoreType.DMA
    out = pl.pallas_call(
        functools.partial(kernel, n, m, plan),
        out_shape=jax.ShapeDtypeStruct((rows, width), bf16),
        in_specs=[hbm] * 8,
        out_specs=pl.BlockSpec(memory_space=pltpu.VMEM),
        scratch_shapes=[
            pltpu.VMEM((rows, width), bf16),
            pltpu.VMEM((1, width), f32),
            pltpu.VMEM(conv_gate.shape, f32),
            pltpu.VMEM(conv_up.shape, f32),
            pltpu.VMEM((1, width), f32),
            pltpu.VMEM((2, chunks, width, 2 * LANES), bf16),
            pltpu.VMEM(w_down.shape, bf16),
            pltpu.VMEM((rows, width), bf16),
            pltpu.VMEM((2, chunks, rows, 2 * LANES), wire),
            pltpu.VMEM((2, chunks, rows, 2 * LANES), wire),
            pltpu.VMEM((rows + 16, 2 * LANES), f32),
            pltpu.VMEM((2, rows, plan.early * LANES), bf16),
            pltpu.VMEM((2, rows, half - plan.early * LANES), bf16),
            pltpu.VMEM((rows, width), f32),
            pltpu.VMEM((8, rows), f32),
            pltpu.VMEM((n, 8, rows), f32),
            pltpu.VMEM((rows, LANES), f32),
            pltpu.VMEM((rows, width), wire),
            pltpu.VMEM((blocks, m, own_rows, width), wire),
            pltpu.VMEM((blocks, own_rows, LANES), f32),
            pltpu.VMEM((blocks, n, own_rows, LANES), f32),
            dma((parts + 4,)), dma((2, 2, chunks)), dma,
            dma((2, chunks, parts)), dma((2, chunks, parts)), dma((2, 2, blocks)), dma((2, 2, blocks)),
            dma((2,)), dma((n,)), dma((blocks, m)), dma((blocks, m)), dma((blocks, n)), dma((blocks, n)),
            dma((blocks, m)), dma((blocks, m)),
        ],
        compiler_params=pltpu.CompilerParams(
            collective_id=0, has_side_effects=True, vmem_limit_bytes=60 * 1024 * 1024
        ),
    )(tokens[0], pre_gain[None], w_gate, w_up, conv_gate, conv_up, w_down, post_gain[None])
    return out[None]


def solution(mesh):
    in_specs = (
        P("dp", None, "ra"),
        P("ra"),
        P("ra", "cb"),
        P("ra", "cb"),
        P(None, "cb"),
        P(None, "cb"),
        P("cb", "ra"),
        P("ra"),
    )
    out_specs = P("dp", None, "ra")
    return jax.shard_map(
        functools.partial(local, mesh.shape["ra"], mesh.shape["cb"]),
        mesh=mesh, in_specs=in_specs, out_specs=out_specs, check_vma=False,
    )
```

time: 150 us -> 136 us (0.907)
  Pallas kernels: 147 us -> 133 us
    pallas_call x1, Pallas kernels: 147 us -> 133 us  [local(): pl.pallas_call(functools.partial(kernel, n, m, plan), out_shape=jax.Shape...]
where the time goes in v1:
time: 136 us
  Pallas kernels  133 us (98%)
  local copies, waits for them, and re-layouts  2.26 us (2%)
    pallas_call x1, Pallas kernels, local(): pl.pallas_call(functools.partial(kernel, n, m, plan), out_shape=jax.Shape...  133 us

profile of v1, /device:TPU:0, one launch (start us, length us, event | category | flops | bytes accessed | tf_op | source)
XLA Modules:
  0.0 135.7 jit_solution(4093826714770470060)
XLA Ops:
  0.0 133.4 %shard_map.82 = bf16[512,1024]{1,0:T(8,128)(2,1)} custom-call(bf16[512,1024]{1,0:T(8,128)(2,1)} %bitcast.5, f32[1,1024]{1,0:T(1,128)} %bitcast.6, bf16[1024,2816]{1,0:T(8,128)(2,1)} %wg_hbm.1, bf16[1024,2816]{1,0:T(8,128)(2,1)} %wu_hbm.1, f32[3,2816]{1,0:T(4,128)} %cg_hbm.1, f32[3,2816]{1,0:T(4,128)} %cu_hbm.1, bf16[2816,1024]{1,0:T(8,128)(2,1)} %wd_hbm.1, ...), custom_call_target="tpu_custom_call" | custom-call | tf_op jit(solution)/shard_map/pallas_call | solution.py:403
  133.4 2.3 %copy.10 = bf16[1,512,1024]{2,1,0:T(8,128)(2,1)} copy(bf16[1,512,1024]{2,1,0:T(8,128)(2,1)} %bitcast.4) | data formatting | bytes 2097152

commit v2 on v1

v2 whole, which is shorter than its diff:
```python
import functools
import jax
import jax.numpy as jnp
from jax import lax
from jax.experimental import pallas as pl
from jax.experimental.pallas import tpu as pltpu
from jax.sharding import PartitionSpec as P

epsilon = 1e-06
residual_scale = 0.125
LANES = 128
PART = 128
BLOCK = 64
LAG = 3
LAST_LAG = 5
FIRST = 32
MESH = pl.DeviceIdType.MESH


def gelu(v):
    return 0.5 * v * (1.0 + jnp.tanh(0.7978845608028654 * (v + 0.044715 * v * v * v)))


class Plan:
    def __init__(self, n, rows, chunks):
        self.parts = rows // PART
        self.blocks = rows // BLOCK
        self.partials = chunks * self.parts
        cuts = (0, (chunks * 3) // 11, (chunks * 7) // 11, chunks)
        self.groups = []
        at = self.partials
        for g in range(3):
            size, lag = (BLOCK, LAG) if g < 2 else (BLOCK // 2, LAST_LAG)
            at = max(at, cuts[g + 1] * self.parts - 1 + LAG * (n - 1))
            self.groups.append((cuts[g], cuts[g + 1], size, rows // size, lag, at))
            at += rows // size
        self.done = self.groups[2][5] + 1
        self.sum_after = 8
        self.slots = self.done + LAST_LAG * (n - 1) + self.sum_after + 2 * self.blocks


def kernel(
    n, m, plan,
    tok_hbm, pre_hbm, wg_hbm, wu_hbm, cg_hbm, cu_hbm, wd_hbm, branch_ref, stat_ref,
    tok, pre, cg, cu,
    w, wd, xw, rbuf, sbuf, full, hid_a, hid_b, hid_c, acc, sq_own, sq_out, sq_in, scale, bsend, brecv, bout, stat,
    lsem, wsem, dsem, psend, pfirst, precv, hsend, hrecv, sqs, sqr, bss, bsr, oss, osr, osl, sts, str_, stl,
):
    rows, width = tok.shape
    wire = sbuf.dtype
    chunks = w.shape[1]
    half = chunks * LANES
    parts, blocks = plan.parts, plan.blocks
    hids = (hid_a, hid_b, hid_c)
    own_rows = BLOCK // m
    dim_full = width * n
    r = lax.axis_index("ra")
    me = lax.axis_index("cb")
    f32, bf16 = jnp.float32, jnp.bfloat16
    upper = (2 * r) // n

    def place(d):
        return r * (1 - d) + (n - 1 - r) * d

    def onward(d):
        return {"ra": (r + 1 - 2 * d + n) % n}

    def somewhere(i, k):
        return {"ra": (r + i) % n, "cb": (me + k) % m}

    def weight_copies(d, c):
        at = pl.ds(pl.multiple_of(d * half + c * LANES, LANES), LANES)
        return (
            pltpu.make_async_copy(wg_hbm.at[:, at], w.at[d, c, :, pl.ds(0, LANES)], wsem.at[0, d, c]),
            pltpu.make_async_copy(wu_hbm.at[:, at], w.at[d, c, :, pl.ds(LANES, LANES)], wsem.at[1, d, c]),
        )

    tok_copies = [
        pltpu.make_async_copy(tok_hbm.at[pl.ds(q * PART, PART)], tok.at[pl.ds(q * PART, PART)], lsem.at[q])
        for q in range(parts)
    ]
    pre_copy = pltpu.make_async_copy(pre_hbm, pre, lsem.at[parts])
    rest = [
        pltpu.make_async_copy(cg_hbm, cg, lsem.at[parts + 1]),
        pltpu.make_async_copy(cu_hbm, cu, lsem.at[parts + 2]),
    ]
    pre_copy.start()
    tok_copies[0].start()
    for d in (0, 1):
        for copy in weight_copies(d, 0):
            copy.start()
    for copy in tok_copies[1:]:
        copy.start()

    barrier = pltpu.get_barrier_semaphore()
    others = [(i, k) for k in range(m) for i in range(n) if i or k]

    for d in (0, 1):
        @pl.when(place(d) < n - 1)
        def _():
            pl.semaphore_signal(barrier, inc=1, device_id=onward(d), device_id_type=MESH)

    for k in range(1, m):
        pl.semaphore_signal(barrier, inc=1, device_id=somewhere(0, k), device_id_type=MESH)

    for copy in rest:
        copy.start()

    down_copy = pltpu.make_async_copy(wd_hbm, wd, dsem)

    def fetch(c):
        for d in (0, 1):
            for copy in weight_copies(d, c):
                copy.start()

    fetch(1)
    full[pl.ds(0, 8), :] = jnp.zeros((8, 2 * LANES), f32)
    full[pl.ds(rows + 8, 8), :] = jnp.zeros((8, 2 * LANES), f32)
    scale[pl.ds(0, 8), :] = jnp.zeros((8, LANES), f32)
    scale[pl.ds(rows + 8, 8), :] = jnp.zeros((8, LANES), f32)

    def square_copy(d):
        return pltpu.make_async_remote_copy(
            src_ref=sq_out.at[d], dst_ref=sq_in.at[d],
            send_sem=sqs.at[d], recv_sem=sqr.at[d],
            device_id=onward(d), device_id_type=MESH,
        )

    def own_squares():
        values = tok[...].astype(f32)
        square = values * values
        high = square.astype(bf16)
        low = (square - high.astype(f32)).astype(bf16)
        ones = jnp.ones((8, width), bf16)
        nt = (((1,), (1,)), ((), ()))
        sq_own[...] = lax.dot_general(ones, high, nt, preferred_element_type=f32) + lax.dot_general(
            ones, low, nt, preferred_element_type=f32
        )

    def square_step(d):
        p = place(d)

        @pl.when(p == 0)
        def _():
            sq_out[d] = sq_own[...]

        @pl.when(p > 0)
        def _():
            square_copy(d).wait_recv()
            sq_out[d] = sq_own[...] + sq_in[d]

        @pl.when(p < n - 1)
        def _():
            square_copy(d).start()

        @pl.when(p == n - 1)
        def _():
            inv = lax.rsqrt(sq_out[d] / dim_full + epsilon)
            scale[pl.ds(8, rows), :] = jnp.concatenate([inv] * (LANES // 8), axis=0).T

    def part_rows(b):
        return pl.ds(pl.multiple_of(b * PART, PART), PART)

    def block_rows(b):
        return pl.ds(pl.multiple_of(b * BLOCK, BLOCK), BLOCK)

    def partial_copy(d, c, b):
        at = part_rows(b)
        return pltpu.make_async_remote_copy(
            src_ref=sbuf.at[d, c, at], dst_ref=rbuf.at[d, c, at],
            send_sem=psend.at[d], recv_sem=precv.at[d, c, b],
            device_id=onward(d), device_id_type=MESH,
        )

    def first_copy(d, b, j):
        at = pl.ds(pl.multiple_of(b * PART + j * FIRST, FIRST), FIRST)
        return pltpu.make_async_remote_copy(
            src_ref=sbuf.at[d, 0, at], dst_ref=rbuf.at[d, 0, at],
            send_sem=psend.at[d], recv_sem=pfirst.at[d, b, j],
            device_id=onward(d), device_id_type=MESH,
        )

    def hidden_copy(d, g, b):
        hid = hids[g]
        size = plan.groups[g][2]
        at = pl.ds(pl.multiple_of(b * size, size), size)
        return pltpu.make_async_remote_copy(
            src_ref=hid.at[1 - d, at], dst_ref=hid.at[1 - d, at],
            send_sem=hsend.at[d, g], recv_sem=hrecv.at[d, g, b],
            device_id=onward(d), device_id_type=MESH,
        )

    def finish_chunk(d, c):
        at = pl.ds(pl.multiple_of(d * half + c * LANES, LANES), LANES)
        taps_g, taps_u = cg[:, at], cu[:, at]
        for j in range(rows // BLOCK):
            by = scale[pl.ds(j * BLOCK, BLOCK + 16), :]
            window = full[pl.ds(j * BLOCK, BLOCK + 16), :] * jnp.concatenate([by, by], axis=1)
            before = pltpu.roll(window, 1, 0)[8:8 + BLOCK]
            here = window[8:8 + BLOCK]
            after = pltpu.roll(window, BLOCK + 15, 0)[8:8 + BLOCK]
            conv = []
            for side, taps in ((0, taps_g), (1, taps_u)):
                lanes = slice(side * LANES, (side + 1) * LANES)
                conv.append(
                    taps[0:1] * before[:, lanes] + taps[1:2] * here[:, lanes] + taps[2:3] * after[:, lanes]
                )
            value = (gelu(conv[0]) * conv[1]).astype(bf16)

            for hid, (low, high, *_) in zip(hids, plan.groups):
                @pl.when((c >= low) & (c < high))
                def _():
                    spot = jnp.clip(c - low, 0, high - low - 1)
                    hid[d, pl.ds(j * BLOCK, BLOCK), pl.ds(pl.multiple_of(spot * LANES, LANES), LANES)] = value

    def partial_step(d, i):
        p = place(d)
        c = i // parts
        b = i % parts
        at = part_rows(b)

        @pl.when(b == 0)
        def _():
            for copy in weight_copies(d, c):
                copy.wait()

        own = jnp.dot(xw[at, :], w[d, c], preferred_element_type=f32)

        @pl.when((p < n - 1) & (c == 0))
        def _():
            for j in range(PART // FIRST):
                some = pl.ds(pl.multiple_of(b * PART + j * FIRST, FIRST), FIRST)
                piece = own[j * FIRST:(j + 1) * FIRST]

                @pl.when(p == 0)
                def _():
                    sbuf[d, 0, some] = piece.astype(wire)

                @pl.when(p > 0)
                def _():
                    first_copy(d, b, j).wait_recv()
                    sbuf[d, 0, some] = (piece + rbuf[d, 0, some].astype(f32)).astype(wire)

                first_copy(d, b, j).start()

        @pl.when((p == 0) & (c > 0))
        def _():
            sbuf[d, c, at] = own.astype(wire)
            partial_copy(d, c, b).start()

        @pl.when((p > 0) & (p < n - 1) & (c > 0))
        def _():
            partial_copy(d, c, b).wait_recv()
            sbuf[d, c, at] = (own + rbuf[d, c, at].astype(f32)).astype(wire)
            partial_copy(d, c, b).start()

        @pl.when(p == n - 1)
        def _():
            @pl.when(c == 0)
            def _():
                for j in range(PART // FIRST):
                    first_copy(d, b, j).wait_recv()

            @pl.when(c > 0)
            def _():
                partial_copy(d, c, b).wait_recv()

            full[pl.ds(pl.multiple_of(b * PART + 8, 8), PART), :] = own + rbuf[d, c, at].astype(f32)

            @pl.when(b == parts - 1)
            def _():
                finish_chunk(d, c)

    def hidden_step(d, g, k):
        p = place(d)
        hid = hids[g]
        low, high, size = plan.groups[g][:3]
        first_row = pl.multiple_of((1 - d) * half + low * LANES, LANES)

        @pl.when(p > 0)
        def _():
            hidden_copy(d, g, k).wait_recv()

        @pl.when((p > 0) & (p < n - 1))
        def _():
            hidden_copy(d, g, k).start()

        every = BLOCK // size

        @pl.when(k % every == every - 1)
        def _():
            at = block_rows(k // every)
            acc[at, :] += jnp.dot(
                hid[1 - d, at, :], wd[pl.ds(first_row, (high - low) * LANES), :],
                preferred_element_type=f32,
            )

    def mine(b):
        return pl.ds(pl.multiple_of(b * BLOCK + me * own_rows, own_rows), own_rows)

    def branch_copy(b, k):
        peer = (me + k) % m
        at = pl.ds(pl.multiple_of(b * BLOCK + peer * own_rows, own_rows), own_rows)
        return pltpu.make_async_remote_copy(
            src_ref=bsend.at[at], dst_ref=brecv.at[k, b],
            send_sem=bss.at[k], recv_sem=bsr.at[b, k],
            device_id={"cb": peer}, device_id_type=MESH,
        )

    def out_copy(b, k):
        return pltpu.make_async_remote_copy(
            src_ref=bout.at[b], dst_ref=branch_ref.at[mine(b)],
            send_sem=oss.at[k], recv_sem=osr.at[k],
            device_id={"cb": (me + k) % m}, device_id_type=MESH,
        )

    def stat_copy(i, k):
        return pltpu.make_async_remote_copy(
            src_ref=stat, dst_ref=stat_ref.at[r * m + me],
            send_sem=sts.at[i, k], recv_sem=str_.at[i, k],
            device_id=somewhere(i, k), device_id_type=MESH,
        )

    keep_stat = pltpu.make_async_copy(stat, stat_ref.at[r * m + me], stl)

    def send_branch(b):
        at = block_rows(b)
        bsend[at, :] = acc[at, :].astype(wire)
        for k in range(1, m):
            branch_copy(b, k).start()

    def sum_branch(b):
        branch = acc[mine(b), :]
        for k in range(1, m):
            branch_copy(b, k).wait_recv()
            branch = branch + brecv[k, b].astype(f32)
        bout[b] = branch.astype(bf16)
        for k in range(1, m):
            out_copy(b, k).start()
        pltpu.make_async_copy(bout.at[b], branch_ref.at[mine(b)], osl).start()
        sums = jnp.sum(branch * branch, axis=1, keepdims=True)
        lanes = stat.shape[1]
        lane = lax.broadcasted_iota(jnp.int32, (own_rows, lanes), 1)
        row = lax.broadcasted_iota(jnp.int32, (own_rows, lanes), 0)
        spread = jnp.sum(jnp.where(lane == b * own_rows + row, sums, 0.0), axis=0, keepdims=True)
        stat[...] = stat[...] + spread

        @pl.when(b == blocks - 1)
        def _():
            for i, k in others:
                stat_copy(i, k).start()
            keep_stat.start()

    pre_copy.wait()

    def slot(s, carry):
        @pl.when(s < parts)
        def _():
            q = jnp.minimum(s, parts - 1)
            at = part_rows(q)
            pltpu.make_async_copy(tok_hbm.at[at], tok.at[at], lsem.at[q]).wait()
            xw[at, :] = (tok[at, :].astype(f32) * pre[...]).astype(bf16)

        @pl.when(s == 0)
        def _():
            pl.semaphore_wait(barrier, jnp.where((r == 0) | (r == n - 1), 1, 2) + m - 1)

        @pl.when(s == parts - 1)
        def _():
            for copy in rest:
                copy.wait()
            own_squares()

        for order in (0, 1):
            d = (order + 1 - upper) % 2
            i = s - LAG * place(d)

            @pl.when(i == parts - 1)
            def _():
                square_step(d)

            @pl.when((i >= 0) & (i < plan.partials))
            def _():
                partial_step(d, i)

        @pl.when((s >= 1) & (s < chunks - 1))
        def _():
            fetch(s + 1)

        @pl.when(s == chunks)
        def _():
            down_copy.start()
            acc[...] = jnp.zeros_like(acc)
            stat[...] = jnp.zeros_like(stat)

        @pl.when(s == plan.partials)
        def _():
            down_copy.wait()

        for g, (_, _, _, count, lag, first) in enumerate(plan.groups):
            for order in (0, 1):
                d = (order + 1 - upper) % 2
                k = s - lag * place(d) - first

                @pl.when((k == 0) & (place(d) == 0))
                def _():
                    def send(j, carry):
                        hidden_copy(d, g, j).start()
                        return carry

                    lax.fori_loop(0, count, send, 0)

                @pl.when((k >= 0) & (k < count))
                def _():
                    hidden_step(d, g, k)

        @pl.when(s == plan.done)
        def _():
            for d in (0, 1):
                @pl.when(place(d) < n - 1)
                def _():
                    pltpu.make_async_remote_copy(
                        src_ref=sbuf.at[d], dst_ref=rbuf.at[d], send_sem=psend.at[d], recv_sem=precv.at[d, 0, 0],
                        device_id=onward(d), device_id_type=MESH,
                    ).wait_send()

        since = s - plan.done - LAST_LAG * jnp.maximum(r, n - 1 - r)
        send_at = since // 2

        @pl.when((since >= 0) & (since % 2 == 0) & (send_at < blocks))
        def _():
            send_branch(send_at)

        since = since - plan.sum_after
        sum_at = since // 2

        @pl.when((since >= 0) & (since % 2 == 0) & (sum_at < blocks))
        def _():
            sum_branch(sum_at)

        return carry

    lax.fori_loop(0, plan.slots, slot, 0)

    for d in (0, 1):
        @pl.when(place(d) < n - 1)
        def _():
            square_copy(d).wait_send()

    for d in (0, 1):
        @pl.when(place(d) < n - 1)
        def _():
            for g in range(3):
                pltpu.make_async_remote_copy(
                    src_ref=hids[g].at[1 - d], dst_ref=hids[g].at[1 - d], send_sem=hsend.at[d, g], recv_sem=hrecv.at[d, g, 0],
                    device_id=onward(d), device_id_type=MESH,
                ).wait_send()

    for k in range(1, m):
        peer = {"cb": (me + k) % m}
        pltpu.make_async_remote_copy(
            src_ref=brecv.at[k], dst_ref=brecv.at[k], send_sem=bss.at[k], recv_sem=bsr.at[0, k],
            device_id=peer, device_id_type=MESH,
        ).wait_send()
        share = branch_ref.at[pl.ds(0, rows // m)]
        pltpu.make_async_remote_copy(
            src_ref=bout, dst_ref=bout, send_sem=oss.at[k], recv_sem=osr.at[k],
            device_id=peer, device_id_type=MESH,
        ).wait_send()
        pltpu.make_async_remote_copy(
            src_ref=share, dst_ref=share, send_sem=oss.at[k], recv_sem=osr.at[k],
            device_id=peer, device_id_type=MESH,
        ).wait_recv()
    share = branch_ref.at[pl.ds(0, rows // m)]
    pltpu.make_async_copy(share, share, osl).wait()
    for i, k in others:
        stat_copy(i, k).wait()
    keep_stat.wait()


def finish_kernel(
    n, m, tok_hbm, branch_hbm, stat_hbm, post_hbm, out_hbm,
    tok, branch, stat, post, scale, out, isem, osem,
):
    rows, width = tok.shape
    parts = rows // PART
    blocks = rows // BLOCK
    own_rows = BLOCK // m
    f32 = jnp.float32
    stat_copy = pltpu.make_async_copy(stat_hbm, stat, isem.at[2 * parts])
    post_copy = pltpu.make_async_copy(post_hbm, post, isem.at[2 * parts + 1])
    stat_copy.start()
    post_copy.start()
    copies = []
    for q in range(parts):
        at = pl.ds(q * PART, PART)
        pair = (
            pltpu.make_async_copy(branch_hbm.at[at], branch.at[at], isem.at[q]),
            pltpu.make_async_copy(tok_hbm.at[at], tok.at[at], isem.at[parts + q]),
        )
        for copy in pair:
            copy.start()
        copies.append(pair)
    stat_copy.wait()
    for k in range(m):
        total = stat[k]
        for i in range(1, n):
            total = total + stat[i * m + k]
        inv = lax.rsqrt(total / (width * n) + epsilon)
        column = jnp.broadcast_to(inv, (LANES, rows // m)).T
        for b in range(blocks):
            scale[pl.ds(b * BLOCK + k * own_rows, own_rows), :] = column[b * own_rows:(b + 1) * own_rows]
    post_copy.wait()
    writes = []
    for q in range(parts):
        for copy in copies[q]:
            copy.wait()
        at = pl.ds(q * PART, PART)
        by = scale[at, :]
        for t in range(width // LANES):
            lanes = pl.ds(t * LANES, LANES)
            mixed = residual_scale * tok[at, lanes].astype(f32) + branch[at, lanes].astype(f32) * by * post[:, lanes]
            out[at, lanes] = mixed.astype(out.dtype)
        write = pltpu.make_async_copy(out.at[at], out_hbm.at[at], osem.at[q])
        write.start()
        writes.append(write)
    for write in writes:
        write.wait()


def local(n, m, tokens, pre_gain, w_gate, w_up, conv_gate, conv_up, w_down, post_gain):
    rows, width = tokens.shape[1:]
    chunks = w_gate.shape[1] // (2 * LANES)
    plan = Plan(n, rows, chunks)
    parts, blocks = plan.parts, plan.blocks
    own_rows = BLOCK // m
    wire = jnp.bfloat16 if n <= 4 else jnp.float32
    f32, bf16 = jnp.float32, jnp.bfloat16
    hbm = pl.BlockSpec(memory_space=pl.ANY)
    dma = pltpu.SemaphoreType.DMA
    branch, stat = pl.pallas_call(
        functools.partial(kernel, n, m, plan),
        out_shape=[
            jax.ShapeDtypeStruct((rows, width), bf16),
            jax.ShapeDtypeStruct((n * m, 1, rows // m), f32),
        ],
        in_specs=[hbm] * 7,
        out_specs=[hbm] * 2,
        scratch_shapes=[
            pltpu.VMEM((rows, width), bf16),
            pltpu.VMEM((1, width), f32),
            pltpu.VMEM(conv_gate.shape, f32),
            pltpu.VMEM(conv_up.shape, f32),
            pltpu.VMEM((2, chunks, width, 2 * LANES), bf16),
            pltpu.VMEM(w_down.shape, bf16),
            pltpu.VMEM((rows, width), bf16),
            pltpu.VMEM((2, chunks, rows, 2 * LANES), wire),
            pltpu.VMEM((2, chunks, rows, 2 * LANES), wire),
            pltpu.VMEM((rows + 16, 2 * LANES), f32),
            *[pltpu.VMEM((2, rows, (high - low) * LANES), bf16) for low, high, *_ in plan.groups],
            pltpu.VMEM((rows, width), f32),
            pltpu.VMEM((8, rows), f32),
            pltpu.VMEM((2, 8, rows), f32),
            pltpu.VMEM((2, 8, rows), f32),
            pltpu.VMEM((rows + 16, LANES), f32),
            pltpu.VMEM((rows, width), wire),
            pltpu.VMEM((m, blocks, own_rows, width), wire),
            pltpu.VMEM((blocks, own_rows, width), bf16),
            pltpu.VMEM((1, rows // m), f32),
            dma((parts + 3,)), dma((2, 2, chunks)), dma,
            dma((2,)), dma((2, parts, PART // FIRST)), dma((2, chunks, parts)), dma((2, 3)), dma((2, 3, 2 * blocks)),
            dma((2,)), dma((2,)), dma((m,)), dma((blocks, m)), dma((m,)), dma((m,)), dma,
            dma((n, m)), dma((n, m)), dma,
        ],
        compiler_params=pltpu.CompilerParams(
            collective_id=0, has_side_effects=True, vmem_limit_bytes=60 * 1024 * 1024
        ),
    )(tokens[0], pre_gain[None], w_gate, w_up, conv_gate, conv_up, w_down)
    out = pl.pallas_call(
        functools.partial(finish_kernel, n, m),
        out_shape=jax.ShapeDtypeStruct((rows, width), bf16),
        in_specs=[hbm] * 4,
        out_specs=hbm,
        scratch_shapes=[
            pltpu.VMEM((rows, width), bf16),
            pltpu.VMEM((rows, width), bf16),
            pltpu.VMEM((n * m, 1, rows // m), f32),
            pltpu.VMEM((1, width), f32),
            pltpu.VMEM((rows, LANES), f32),
            pltpu.VMEM((rows, width), bf16),
            dma((2 * parts + 2,)), dma((parts,)),
        ],
    )(tokens[0], branch, stat, post_gain[None])
    return out[None]


def solution(mesh):
    in_specs = (
        P("dp", None, "ra"),
        P("ra"),
        P("ra", "cb"),
        P("ra", "cb"),
        P(None, "cb"),
        P(None, "cb"),
        P("cb", "ra"),
        P("ra"),
    )
    out_specs = P("dp", None, "ra")
    return jax.shard_map(
        functools.partial(local, mesh.shape["ra"], mesh.shape["cb"]),
        mesh=mesh, in_specs=in_specs, out_specs=out_specs, check_vma=False,
    )
```

time: 136 us -> 131 us (0.963)
  Pallas kernels: 133 us -> 130 us
  local copies, waits for them, and re-layouts: 2.26 us -> 0 us
    pallas_call x1 -> x2, Pallas kernels: 133 us -> 130 us  [the longest x1 128 us: local(): pl.pallas_call(functools.partial(kernel, n, m, plan), out_shape=[jax.Shap...]
    unnamed x1 -> x0, local copies, waits for them, and re-layouts: 2.26 us -> none
where the time goes in v2:
time: 131 us; the launch traced here: 130 us
  Pallas kernels  130 us (99%)
    pallas_call x1, Pallas kernels, local(): pl.pallas_call(functools.partial(kernel, n, m, plan), out_shape=[jax.Shap...  128 us

profile of v2, /device:TPU:0, one launch (start us, length us, event | category | flops | bytes accessed | tf_op | source)
XLA Modules:
  0.0 130.5 jit_solution(6110224880821555280)
XLA Ops:
  0.0 128.0 %shard_map.82 = (bf16[512,1024]{1,0:T(8,128)(2,1)}, f32[16,1,128]{2,1,0:T(1,128)}) custom-call(bf16[512,1024]{1,0:T(8,128)(2,1)} %bitcast.4, f32[1,1024]{1,0:T(1,128)} %bitcast.7, bf16[1024,2816]{1,0:T(8,128)(2,1)} %wg_hbm.1, bf16[1024,2816]{1,0:T(8,128)(2,1)} %wu_hbm.1, f32[3,2816]{1,0:T(4,128)} %cg_hbm.1, f32[3,2816]{1,0:T(4,128)} %cu_hbm.1, ...), custom_call_target="tpu_custom_call" | custom-call | tf_op jit(solution)/shard_map/pallas_call | solution.py:541
  128.0 2.5 %shard_map.83 = bf16[512,1024]{1,0:T(8,128)(2,1)} custom-call(bf16[512,1024]{1,0:T(8,128)(2,1)} %bitcast.5, bf16[512,1024]{1,0:T(8,128)(2,1)} %get-tuple-element.7.branch_hbm, f32[16,1,128]{2,1,0:T(1,128)} %get-tuple-element.8.stat_hbm, f32[1,1024]{1,0:T(1,128)} %bitcast.6), custom_call_target="tpu_custom_call" | custom-call | tf_op jit(solution)/shard_map/pallas_call | solution.py:579

commit v3 on v2

--- a/solution.py
+++ b/solution.py
@@ -11,9 +11,12 @@
 LANES = 128
 PART = 128
 BLOCK = 64
+STRIPE = 16
 LAG = 3
-LAST_LAG = 5
+ROW_LAG = 4
+LEAD = 5
 FIRST = 32
+PIECE = 32
 MESH = pl.DeviceIdType.MESH
 
 
@@ -24,34 +27,33 @@
 class Plan:
     def __init__(self, n, rows, chunks):
         self.parts = rows // PART
+        self.head = self.parts - 1
         self.blocks = rows // BLOCK
+        self.upper = chunks * self.head
         self.partials = chunks * self.parts
-        cuts = (0, (chunks * 3) // 11, (chunks * 7) // 11, chunks)
-        self.groups = []
-        at = self.partials
-        for g in range(3):
-            size, lag = (BLOCK, LAG) if g < 2 else (BLOCK // 2, LAST_LAG)
-            at = max(at, cuts[g + 1] * self.parts - 1 + LAG * (n - 1))
-            self.groups.append((cuts[g], cuts[g + 1], size, rows // size, lag, at))
-            at += rows // size
-        self.done = self.groups[2][5] + 1
-        self.sum_after = 8
-        self.slots = self.done + LAST_LAG * (n - 1) + self.sum_after + 2 * self.blocks
+        self.cut = self.head * PART - PIECE
+        self.stripes = rows // STRIPE
+        self.early = self.cut // STRIPE
+        reach = LAG * (n - 1)
+        self.a = max(self.partials, self.upper - 1 + reach)
+        self.b = max(self.a + self.early, self.partials - 1 + reach + LEAD)
+        self.ring = ROW_LAG * (n - 1) + LEAD + 3
+        self.sum_after = 6
+        self.slots = self.b + self.stripes - self.early + ROW_LAG * (n - 1) + self.sum_after
 
 
 def kernel(
     n, m, plan,
     tok_hbm, pre_hbm, wg_hbm, wu_hbm, cg_hbm, cu_hbm, wd_hbm, branch_ref, stat_ref,
     tok, pre, cg, cu,
-    w, wd, xw, rbuf, sbuf, full, hid_a, hid_b, hid_c, acc, sq_own, sq_out, sq_in, scale, bsend, brecv, bout, stat,
-    lsem, wsem, dsem, psend, pfirst, precv, hsend, hrecv, sqs, sqr, bss, bsr, oss, osr, osl, sts, str_, stl,
+    w, wd, xw, rbuf, sbuf, full, hid, acc, sq_own, sq_out, sq_in, scale, bsend, brecv, bout, stat,
+    lsem, wsem, dsem, psend, pfirst, ring, hsend, sqs, sqr, bss, bsr, oss, osr, osl, sts, str_, stl,
 ):
     rows, width = tok.shape
     wire = sbuf.dtype
-    chunks = w.shape[1]
+    chunks = w.shape[0]
     half = chunks * LANES
     parts, blocks = plan.parts, plan.blocks
-    hids = (hid_a, hid_b, hid_c)
     own_rows = BLOCK // m
     dim_full = width * n
     r = lax.axis_index("ra")
@@ -71,8 +73,8 @@
     def weight_copies(d, c):
         at = pl.ds(pl.multiple_of(d * half + c * LANES, LANES), LANES)
         return (
-            pltpu.make_async_copy(wg_hbm.at[:, at], w.at[d, c, :, pl.ds(0, LANES)], wsem.at[0, d, c]),
-            pltpu.make_async_copy(wu_hbm.at[:, at], w.at[d, c, :, pl.ds(LANES, LANES)], wsem.at[1, d, c]),
+            pltpu.make_async_copy(wg_hbm.at[:, at], w.at[c, d, :, pl.ds(0, LANES)], wsem.at[c]),
+            pltpu.make_async_copy(wu_hbm.at[:, at], w.at[c, d, :, pl.ds(LANES, LANES)], wsem.at[c]),
         )
 
     tok_copies = [
@@ -114,8 +116,9 @@
                 copy.start()
 
     fetch(1)
-    full[pl.ds(0, 8), :] = jnp.zeros((8, 2 * LANES), f32)
-    full[pl.ds(rows + 8, 8), :] = jnp.zeros((8, 2 * LANES), f32)
+    for c in range(chunks):
+        full[c, pl.ds(0, 8), :] = jnp.zeros((8, 2 * LANES), f32)
+        full[c, pl.ds(rows + 8, 8), :] = jnp.zeros((8, 2 * LANES), f32)
     scale[pl.ds(0, 8), :] = jnp.zeros((8, LANES), f32)
     scale[pl.ds(rows + 8, 8), :] = jnp.zeros((8, LANES), f32)
 
@@ -164,72 +167,59 @@
     def block_rows(b):
         return pl.ds(pl.multiple_of(b * BLOCK, BLOCK), BLOCK)
 
-    def partial_copy(d, c, b):
+    def partial_copy(d, i, c, b):
         at = part_rows(b)
         return pltpu.make_async_remote_copy(
             src_ref=sbuf.at[d, c, at], dst_ref=rbuf.at[d, c, at],
-            send_sem=psend.at[d], recv_sem=precv.at[d, c, b],
+            send_sem=psend.at[d], recv_sem=ring.at[d, i % plan.ring],
             device_id=onward(d), device_id_type=MESH,
         )
 
-    def first_copy(d, b, j):
-        at = pl.ds(pl.multiple_of(b * PART + j * FIRST, FIRST), FIRST)
+    def first_copy(d, j):
+        at = pl.ds(j * FIRST, FIRST)
         return pltpu.make_async_remote_copy(
             src_ref=sbuf.at[d, 0, at], dst_ref=rbuf.at[d, 0, at],
-            send_sem=psend.at[d], recv_sem=pfirst.at[d, b, j],
+            send_sem=psend.at[d], recv_sem=pfirst.at[d, j],
             device_id=onward(d), device_id_type=MESH,
         )
 
-    def hidden_copy(d, g, b):
-        hid = hids[g]
-        size = plan.groups[g][2]
-        at = pl.ds(pl.multiple_of(b * size, size), size)
+    def hidden_copy(d, k):
+        at = pl.ds(pl.multiple_of(k * STRIPE, STRIPE), STRIPE)
         return pltpu.make_async_remote_copy(
             src_ref=hid.at[1 - d, at], dst_ref=hid.at[1 - d, at],
-            send_sem=hsend.at[d, g], recv_sem=hrecv.at[d, g, b],
+            send_sem=hsend.at[d], recv_sem=ring.at[d, (plan.partials + k) % plan.ring],
             device_id=onward(d), device_id_type=MESH,
         )
 
-    def finish_chunk(d, c):
+    def finish_rows(d, c, low, high):
         at = pl.ds(pl.multiple_of(d * half + c * LANES, LANES), LANES)
+        to = pl.ds(pl.multiple_of(c * LANES, LANES), LANES)
         taps_g, taps_u = cg[:, at], cu[:, at]
-        for j in range(rows // BLOCK):
-            by = scale[pl.ds(j * BLOCK, BLOCK + 16), :]
-            window = full[pl.ds(j * BLOCK, BLOCK + 16), :] * jnp.concatenate([by, by], axis=1)
-            before = pltpu.roll(window, 1, 0)[8:8 + BLOCK]
-            here = window[8:8 + BLOCK]
-            after = pltpu.roll(window, BLOCK + 15, 0)[8:8 + BLOCK]
+        for j in range(low, high, PIECE):
+            by = scale[pl.ds(j, PIECE + 16), :]
+            window = full[c, pl.ds(j, PIECE + 16), :] * jnp.concatenate([by, by], axis=1)
+            before = pltpu.roll(window, 1, 0)[8:8 + PIECE]
+            here = window[8:8 + PIECE]
+            after = pltpu.roll(window, PIECE + 15, 0)[8:8 + PIECE]
             conv = []
             for side, taps in ((0, taps_g), (1, taps_u)):
                 lanes = slice(side * LANES, (side + 1) * LANES)
                 conv.append(
                     taps[0:1] * before[:, lanes] + taps[1:2] * here[:, lanes] + taps[2:3] * after[:, lanes]
                 )
-            value = (gelu(conv[0]) * conv[1]).astype(bf16)
-
-            for hid, (low, high, *_) in zip(hids, plan.groups):
-                @pl.when((c >= low) & (c < high))
-                def _():
-                    spot = jnp.clip(c - low, 0, high - low - 1)
-                    hid[d, pl.ds(j * BLOCK, BLOCK), pl.ds(pl.multiple_of(spot * LANES, LANES), LANES)] = value
+            hid[d, pl.ds(j, PIECE), to] = (gelu(conv[0]) * conv[1]).astype(bf16)
 
     def partial_step(d, i):
         p = place(d)
-        c = i // parts
-        b = i % parts
+        c = jnp.where(i < plan.upper, i // plan.head, i - plan.upper)
+        b = jnp.where(i < plan.upper, i % plan.head, plan.head)
         at = part_rows(b)
-
-        @pl.when(b == 0)
-        def _():
-            for copy in weight_copies(d, c):
-                copy.wait()
-
-        own = jnp.dot(xw[at, :], w[d, c], preferred_element_type=f32)
-
-        @pl.when((p < n - 1) & (c == 0))
+        own = jnp.dot(xw[at, :], w[c, d], preferred_element_type=f32)
+
+        @pl.when((p < n - 1) & (i == 0))
         def _():
             for j in range(PART // FIRST):
-                some = pl.ds(pl.multiple_of(b * PART + j * FIRST, FIRST), FIRST)
+                some = pl.ds(j * FIRST, FIRST)
                 piece = own[j * FIRST:(j + 1) * FIRST]
 
                 @pl.when(p == 0)
@@ -238,60 +228,62 @@
 
                 @pl.when(p > 0)
                 def _():
-                    first_copy(d, b, j).wait_recv()
+                    first_copy(d, j).wait_recv()
                     sbuf[d, 0, some] = (piece + rbuf[d, 0, some].astype(f32)).astype(wire)
 
-                first_copy(d, b, j).start()
-
-        @pl.when((p == 0) & (c > 0))
+                first_copy(d, j).start()
+
+        @pl.when((p == 0) & (i > 0))
         def _():
             sbuf[d, c, at] = own.astype(wire)
-            partial_copy(d, c, b).start()
-
-        @pl.when((p > 0) & (p < n - 1) & (c > 0))
-        def _():
-            partial_copy(d, c, b).wait_recv()
+            partial_copy(d, i, c, b).start()
+
+        @pl.when((p > 0) & (p < n - 1) & (i > 0))
+        def _():
+            partial_copy(d, i, c, b).wait_recv()
             sbuf[d, c, at] = (own + rbuf[d, c, at].astype(f32)).astype(wire)
-            partial_copy(d, c, b).start()
+            partial_copy(d, i, c, b).start()
 
         @pl.when(p == n - 1)
         def _():
-            @pl.when(c == 0)
+            @pl.when(i == 0)
             def _():
                 for j in range(PART // FIRST):
-                    first_copy(d, b, j).wait_recv()
-
-            @pl.when(c > 0)
-            def _():
-                partial_copy(d, c, b).wait_recv()
-
-            full[pl.ds(pl.multiple_of(b * PART + 8, 8), PART), :] = own + rbuf[d, c, at].astype(f32)
-
-            @pl.when(b == parts - 1)
-            def _():
-                finish_chunk(d, c)
-
-    def hidden_step(d, g, k):
+                    first_copy(d, j).wait_recv()
+
+            @pl.when(i > 0)
+            def _():
+                partial_copy(d, i, c, b).wait_recv()
+
+            full[c, pl.ds(pl.multiple_of(b * PART + 8, 8), PART), :] = own + rbuf[d, c, at].astype(f32)
+
+            @pl.when(b == plan.head - 1)
+            def _():
+                finish_rows(d, c, 0, plan.cut)
+
+            @pl.when(b == plan.head)
+            def _():
+                finish_rows(d, c, plan.cut, rows)
+
+    def hidden_pass(d, k):
         p = place(d)
-        hid = hids[g]
-        low, high, size = plan.groups[g][:3]
-        first_row = pl.multiple_of((1 - d) * half + low * LANES, LANES)
 
         @pl.when(p > 0)
         def _():
-            hidden_copy(d, g, k).wait_recv()
+            hidden_copy(d, k).wait_recv()
 
         @pl.when((p > 0) & (p < n - 1))
         def _():
-            hidden_copy(d, g, k).start()
-
-        every = BLOCK // size
+            hidden_copy(d, k).start()
+
+    def hidden_use(d, k):
+        every = BLOCK // STRIPE
 
         @pl.when(k % every == every - 1)
         def _():
             at = block_rows(k // every)
             acc[at, :] += jnp.dot(
-                hid[1 - d, at, :], wd[pl.ds(first_row, (high - low) * LANES), :],
+                hid[1 - d, at, :], wd[pl.ds(pl.multiple_of((1 - d) * half, LANES), half), :],
                 preferred_element_type=f32,
             )
 
@@ -302,8 +294,8 @@
         peer = (me + k) % m
         at = pl.ds(pl.multiple_of(b * BLOCK + peer * own_rows, own_rows), own_rows)
         return pltpu.make_async_remote_copy(
-            src_ref=bsend.at[at], dst_ref=brecv.at[k, b],
-            send_sem=bss.at[k], recv_sem=bsr.at[b, k],
+            src_ref=bsend.at[at], dst_ref=brecv.at[b, k],
+            send_sem=bss.at[k], recv_sem=bsr.at[b],
             device_id={"cb": peer}, device_id_type=MESH,
         )
 
@@ -317,7 +309,7 @@
     def stat_copy(i, k):
         return pltpu.make_async_remote_copy(
             src_ref=stat, dst_ref=stat_ref.at[r * m + me],
-            send_sem=sts.at[i, k], recv_sem=str_.at[i, k],
+            send_sem=sts, recv_sem=str_,
             device_id=somewhere(i, k), device_id_type=MESH,
         )
 
@@ -331,9 +323,10 @@
 
     def sum_branch(b):
         branch = acc[mine(b), :]
+        incoming = brecv.at[b, pl.ds(1, m - 1)]
+        pltpu.make_async_copy(incoming, incoming, bsr.at[b]).wait()
         for k in range(1, m):
-            branch_copy(b, k).wait_recv()
-            branch = branch + brecv[k, b].astype(f32)
+            branch = branch + brecv[b, k].astype(f32)
         bout[b] = branch.astype(bf16)
         for k in range(1, m):
             out_copy(b, k).start()
@@ -354,28 +347,38 @@
     pre_copy.wait()
 
     def slot(s, carry):
-        @pl.when(s < parts)
-        def _():
-            q = jnp.minimum(s, parts - 1)
+        def take(q):
             at = part_rows(q)
             pltpu.make_async_copy(tok_hbm.at[at], tok.at[at], lsem.at[q]).wait()
             xw[at, :] = (tok[at, :].astype(f32) * pre[...]).astype(bf16)
 
+        @pl.when(s < plan.head)
+        def _():
+            take(jnp.minimum(s, parts - 1))
+
         @pl.when(s == 0)
         def _():
             pl.semaphore_wait(barrier, jnp.where((r == 0) | (r == n - 1), 1, 2) + m - 1)
 
-        @pl.when(s == parts - 1)
-        def _():
+        @pl.when(s == plan.head - 1)
+        def _():
+            take(plan.head)
             for copy in rest:
                 copy.wait()
             own_squares()
 
+        t = s - LAG * jnp.minimum(r, n - 1 - r)
+
+        @pl.when((t >= 0) & (t < plan.upper) & (t % plan.head == 0))
+        def _():
+            c = t // plan.head
+            pltpu.make_async_copy(w.at[c], w.at[c], wsem.at[c]).wait()
+
         for order in (0, 1):
             d = (order + 1 - upper) % 2
             i = s - LAG * place(d)
 
-            @pl.when(i == parts - 1)
+            @pl.when(i == plan.head - 1)
             def _():
                 square_step(d)
 
@@ -397,46 +400,56 @@
         def _():
             down_copy.wait()
 
-        for g, (_, _, _, count, lag, first) in enumerate(plan.groups):
+        for order in (0, 1):
+            d = (order + 1 - upper) % 2
+            p = place(d)
+
+            @pl.when((p == 0) & (s == plan.a))
+            def _():
+                def send(j, carry):
+                    hidden_copy(d, j).start()
+                    return carry
+
+                lax.fori_loop(0, LEAD, send, 0)
+
+            ahead = s + LEAD - plan.a
+
+            @pl.when((p == 0) & (s >= plan.a) & (ahead < plan.early))
+            def _():
+                hidden_copy(d, ahead).start()
+
+            ahead = s + LEAD - plan.b
+
+            @pl.when((p == 0) & (ahead >= 0) & (ahead < plan.stripes - plan.early))
+            def _():
+                hidden_copy(d, ahead + plan.early).start()
+
+        def stripe(t):
+            k = jnp.where(t < plan.b, t - plan.a, t - plan.b + plan.early)
+            return k, ((t >= plan.a) & (t < plan.a + plan.early)) | ((t >= plan.b) & (k < plan.stripes))
+
+        for step in (hidden_pass, hidden_use):
             for order in (0, 1):
                 d = (order + 1 - upper) % 2
-                k = s - lag * place(d) - first
-
-                @pl.when((k == 0) & (place(d) == 0))
+                k, live = stripe(s - ROW_LAG * place(d))
+
+                @pl.when(live)
                 def _():
-                    def send(j, carry):
-                        hidden_copy(d, g, j).start()
-                        return carry
-
-                    lax.fori_loop(0, count, send, 0)
-
-                @pl.when((k >= 0) & (k < count))
-                def _():
-                    hidden_step(d, g, k)
-
-        @pl.when(s == plan.done)
-        def _():
-            for d in (0, 1):
-                @pl.when(place(d) < n - 1)
-                def _():
-                    pltpu.make_async_remote_copy(
-                        src_ref=sbuf.at[d], dst_ref=rbuf.at[d], send_sem=psend.at[d], recv_sem=precv.at[d, 0, 0],
-                        device_id=onward(d), device_id_type=MESH,
-                    ).wait_send()
-
-        since = s - plan.done - LAST_LAG * jnp.maximum(r, n - 1 - r)
-        send_at = since // 2
-
-        @pl.when((since >= 0) & (since % 2 == 0) & (send_at < blocks))
-        def _():
-            send_branch(send_at)
-
-        since = since - plan.sum_after
-        sum_at = since // 2
-
-        @pl.when((since >= 0) & (since % 2 == 0) & (sum_at < blocks))
-        def _():
-            sum_branch(sum_at)
+                    step(d, k)
+
+        every = BLOCK // STRIPE
+        done = s - ROW_LAG * jnp.maximum(r, n - 1 - r)
+        send_at, live = stripe(done)
+
+        @pl.when(live & (send_at % every == every - 1))
+        def _():
+            send_branch(send_at // every)
+
+        sum_at, live = stripe(done - plan.sum_after)
+
+        @pl.when(live & (sum_at % every == every - 1))
+        def _():
+            sum_branch(sum_at // every)
 
         return carry
 
@@ -446,20 +459,17 @@
         @pl.when(place(d) < n - 1)
         def _():
             square_copy(d).wait_send()
-
-    for d in (0, 1):
-        @pl.when(place(d) < n - 1)
-        def _():
-            for g in range(3):
+            for buffer, sem in ((sbuf.at[d], psend.at[d]), (hid.at[1 - d], hsend.at[d])):
                 pltpu.make_async_remote_copy(
-                    src_ref=hids[g].at[1 - d], dst_ref=hids[g].at[1 - d], send_sem=hsend.at[d, g], recv_sem=hrecv.at[d, g, 0],
+                    src_ref=buffer, dst_ref=buffer, send_sem=sem, recv_sem=ring.at[d, 0],
                     device_id=onward(d), device_id_type=MESH,
                 ).wait_send()
 
     for k in range(1, m):
         peer = {"cb": (me + k) % m}
+        sent = brecv.at[:, k]
         pltpu.make_async_remote_copy(
-            src_ref=brecv.at[k], dst_ref=brecv.at[k], send_sem=bss.at[k], recv_sem=bsr.at[0, k],
+            src_ref=sent, dst_ref=sent, send_sem=bss.at[k], recv_sem=bsr.at[0],
             device_id=peer, device_id_type=MESH,
         ).wait_send()
         share = branch_ref.at[pl.ds(0, rows // m)]
@@ -473,8 +483,13 @@
         ).wait_recv()
     share = branch_ref.at[pl.ds(0, rows // m)]
     pltpu.make_async_copy(share, share, osl).wait()
-    for i, k in others:
-        stat_copy(i, k).wait()
+    all_stats = stat_ref.at[pl.ds(0, len(others))]
+    both = pltpu.make_async_remote_copy(
+        src_ref=all_stats, dst_ref=all_stats, send_sem=sts, recv_sem=str_,
+        device_id=somewhere(0, 1), device_id_type=MESH,
+    )
+    both.wait_send()
+    both.wait_recv()
     keep_stat.wait()
 
 
@@ -551,26 +566,26 @@
             pltpu.VMEM((1, width), f32),
             pltpu.VMEM(conv_gate.shape, f32),
             pltpu.VMEM(conv_up.shape, f32),
-            pltpu.VMEM((2, chunks, width, 2 * LANES), bf16),
+            pltpu.VMEM((chunks, 2, width, 2 * LANES), bf16),
             pltpu.VMEM(w_down.shape, bf16),
             pltpu.VMEM((rows, width), bf16),
             pltpu.VMEM((2, chunks, rows, 2 * LANES), wire),
             pltpu.VMEM((2, chunks, rows, 2 * LANES), wire),
-            pltpu.VMEM((rows + 16, 2 * LANES), f32),
-            *[pltpu.VMEM((2, rows, (high - low) * LANES), bf16) for low, high, *_ in plan.groups],
+            pltpu.VMEM((chunks, rows + 16, 2 * LANES), f32),
+            pltpu.VMEM((2, rows, chunks * LANES), bf16),
             pltpu.VMEM((rows, width), f32),
             pltpu.VMEM((8, rows), f32),
             pltpu.VMEM((2, 8, rows), f32),
             pltpu.VMEM((2, 8, rows), f32),
             pltpu.VMEM((rows + 16, LANES), f32),
             pltpu.VMEM((rows, width), wire),
-            pltpu.VMEM((m, blocks, own_rows, width), wire),
+            pltpu.VMEM((blocks, m, own_rows, width), wire),
             pltpu.VMEM((blocks, own_rows, width), bf16),
             pltpu.VMEM((1, rows // m), f32),
-            dma((parts + 3,)), dma((2, 2, chunks)), dma,
-            dma((2,)), dma((2, parts, PART // FIRST)), dma((2, chunks, parts)), dma((2, 3)), dma((2, 3, 2 * blocks)),
-            dma((2,)), dma((2,)), dma((m,)), dma((blocks, m)), dma((m,)), dma((m,)), dma,
-            dma((n, m)), dma((n, m)), dma,
+            dma((parts + 3,)), dma((chunks,)), dma,
+            dma((2,)), dma((2, PART // FIRST)), dma((2, plan.ring)), dma((2,)),
+            dma((2,)), dma((2,)), dma((m,)), dma((blocks,)), dma((m,)), dma((m,)), dma,
+            dma, dma, dma,
         ],
         compiler_params=pltpu.CompilerParams(
             collective_id=0, has_side_effects=True, vmem_limit_bytes=60 * 1024 * 1024

time: 131 us -> 122 us (0.931)
  Pallas kernels: 130 us -> 122 us
    pallas_call x1, Pallas kernels: 128 us -> 119 us  [local(): pl.pallas_call(functools.partial(kernel, n, m, plan), out_shape=[jax.Shap...]
where the time goes in v3:
time: 122 us
  Pallas kernels  122 us (100%)
    pallas_call x1, Pallas kernels, local(): pl.pallas_call(functools.partial(kernel, n, m, plan), out_shape=[jax.Shap...  119 us
    pallas_call x1, Pallas kernels, local(): pl.pallas_call(functools.partial(finish_kernel, n, m), out_shape=jax.Shap...  2.5 us

profile of v3, /device:TPU:0, one launch (start us, length us, event | category | flops | bytes accessed | tf_op | source)
XLA Modules:
  0.0 121.7 jit_solution(17323534762356452485)
XLA Ops:
  0.0 119.2 %shard_map.82 = (bf16[512,1024]{1,0:T(8,128)(2,1)}, f32[16,1,128]{2,1,0:T(1,128)}) custom-call(bf16[512,1024]{1,0:T(8,128)(2,1)} %bitcast.4, f32[1,1024]{1,0:T(1,128)} %bitcast.7, bf16[1024,2816]{1,0:T(8,128)(2,1)} %wg_hbm.1, bf16[1024,2816]{1,0:T(8,128)(2,1)} %wu_hbm.1, f32[3,2816]{1,0:T(4,128)} %cg_hbm.1, f32[3,2816]{1,0:T(4,128)} %cu_hbm.1, ...), custom_call_target="tpu_custom_call" | custom-call | tf_op jit(solution)/shard_map/pallas_call | solution.py:556
  119.2 2.5 %shard_map.83 = bf16[512,1024]{1,0:T(8,128)(2,1)} custom-call(bf16[512,1024]{1,0:T(8,128)(2,1)} %bitcast.5, bf16[512,1024]{1,0:T(8,128)(2,1)} %get-tuple-element.7.branch_hbm, f32[16,1,128]{2,1,0:T(1,128)} %get-tuple-element.8.stat_hbm, f32[1,1024]{1,0:T(1,128)} %bitcast.6), custom_call_target="tpu_custom_call" | custom-call | tf_op jit(solution)/shard_map/pallas_call | solution.py:594

commit v4 on v3

--- a/solution.py
+++ b/solution.py
@@ -28,7 +28,7 @@
     def __init__(self, n, rows, chunks):
         self.parts = rows // PART
         self.head = self.parts - 1
-        self.blocks = rows // BLOCK
+        self.blocks = rows // BLOCK - 1
         self.upper = chunks * self.head
         self.partials = chunks * self.parts
         self.cut = self.head * PART - PIECE
@@ -38,16 +38,17 @@
         self.a = max(self.partials, self.upper - 1 + reach)
         self.b = max(self.a + self.early, self.partials - 1 + reach + LEAD)
         self.ring = ROW_LAG * (n - 1) + LEAD + 3
-        self.sum_after = 6
-        self.slots = self.b + self.stripes - self.early + ROW_LAG * (n - 1) + self.sum_after
+        self.sum_after = 5
+        self.tail = max(self.a, self.partials + reach)
+        self.slots = self.b + self.stripes - self.early + ROW_LAG * (n - 1)
 
 
 def kernel(
     n, m, plan,
     tok_hbm, pre_hbm, wg_hbm, wu_hbm, cg_hbm, cu_hbm, wd_hbm, branch_ref, stat_ref,
     tok, pre, cg, cu,
-    w, wd, xw, rbuf, sbuf, full, hid, acc, sq_own, sq_out, sq_in, scale, bsend, brecv, bout, stat,
-    lsem, wsem, dsem, psend, pfirst, ring, hsend, sqs, sqr, bss, bsr, oss, osr, osl, sts, str_, stl,
+    w, wd, xw, rbuf, sbuf, full, hid, acc, sq_own, sq_out, sq_in, scale, bsend, brecv, bout, hsend_rows, hrecv_rows, hout, stat,
+    lsem, wsem, dsem, psend, pfirst, ring, hsend, sqs, sqr, bss, bsr, oss, osr, osl, hss, hsr, hos, sts, str_, stl,
 ):
     rows, width = tok.shape
     wire = sbuf.dtype
@@ -55,6 +56,7 @@
     half = chunks * LANES
     parts, blocks = plan.parts, plan.blocks
     own_rows = BLOCK // m
+    half_own = own_rows // 2
     dim_full = width * n
     r = lax.axis_index("ra")
     me = lax.axis_index("cb")
@@ -73,8 +75,8 @@
     def weight_copies(d, c):
         at = pl.ds(pl.multiple_of(d * half + c * LANES, LANES), LANES)
         return (
-            pltpu.make_async_copy(wg_hbm.at[:, at], w.at[c, d, :, pl.ds(0, LANES)], wsem.at[c]),
-            pltpu.make_async_copy(wu_hbm.at[:, at], w.at[c, d, :, pl.ds(LANES, LANES)], wsem.at[c]),
+            pltpu.make_async_copy(wg_hbm.at[:, at], w.at[c, d, :, pl.ds(0, LANES)], wsem.at[lax.rem(c, 4)]),
+            pltpu.make_async_copy(wu_hbm.at[:, at], w.at[c, d, :, pl.ds(LANES, LANES)], wsem.at[lax.rem(c, 4)]),
         )
 
     tok_copies = [
@@ -105,22 +107,12 @@
     for k in range(1, m):
         pl.semaphore_signal(barrier, inc=1, device_id=somewhere(0, k), device_id_type=MESH)
 
-    for copy in rest:
-        copy.start()
-
     down_copy = pltpu.make_async_copy(wd_hbm, wd, dsem)
 
     def fetch(c):
         for d in (0, 1):
             for copy in weight_copies(d, c):
                 copy.start()
-
-    fetch(1)
-    for c in range(chunks):
-        full[c, pl.ds(0, 8), :] = jnp.zeros((8, 2 * LANES), f32)
-        full[c, pl.ds(rows + 8, 8), :] = jnp.zeros((8, 2 * LANES), f32)
-    scale[pl.ds(0, 8), :] = jnp.zeros((8, LANES), f32)
-    scale[pl.ds(rows + 8, 8), :] = jnp.zeros((8, LANES), f32)
 
     def square_copy(d):
         return pltpu.make_async_remote_copy(
@@ -171,7 +163,7 @@
         at = part_rows(b)
         return pltpu.make_async_remote_copy(
             src_ref=sbuf.at[d, c, at], dst_ref=rbuf.at[d, c, at],
-            send_sem=psend.at[d], recv_sem=ring.at[d, i % plan.ring],
+            send_sem=psend.at[d], recv_sem=ring.at[d, lax.rem(i, plan.ring)],
             device_id=onward(d), device_id_type=MESH,
         )
 
@@ -187,7 +179,7 @@
         at = pl.ds(pl.multiple_of(k * STRIPE, STRIPE), STRIPE)
         return pltpu.make_async_remote_copy(
             src_ref=hid.at[1 - d, at], dst_ref=hid.at[1 - d, at],
-            send_sem=hsend.at[d], recv_sem=ring.at[d, (plan.partials + k) % plan.ring],
+            send_sem=hsend.at[d], recv_sem=ring.at[d, lax.rem(plan.partials + k, plan.ring)],
             device_id=onward(d), device_id_type=MESH,
         )
 
@@ -211,8 +203,8 @@
 
     def partial_step(d, i):
         p = place(d)
-        c = jnp.where(i < plan.upper, i // plan.head, i - plan.upper)
-        b = jnp.where(i < plan.upper, i % plan.head, plan.head)
+        c = jnp.where(i < plan.upper, lax.div(i, plan.head), i - plan.upper)
+        b = jnp.where(i < plan.upper, lax.rem(i, plan.head), plan.head)
         at = part_rows(b)
         own = jnp.dot(xw[at, :], w[c, d], preferred_element_type=f32)
 
@@ -279,14 +271,27 @@
     def hidden_use(d, k):
         every = BLOCK // STRIPE
 
-        @pl.when(k % every == every - 1)
-        def _():
-            at = block_rows(k // every)
+        def product(at):
             acc[at, :] += jnp.dot(
                 hid[1 - d, at, :], wd[pl.ds(pl.multiple_of((1 - d) * half, LANES), half), :],
                 preferred_element_type=f32,
             )
 
+        @pl.when((lax.rem(k, every) == every - 1) & (k < plan.stripes - every))
+        def _():
+            product(block_rows(lax.div(k, every)))
+
+        ends = place(d) == n - 1
+
+        @pl.when((k == plan.stripes - 1) & jnp.logical_not(ends))
+        def _():
+            product(pl.ds(rows - BLOCK, BLOCK))
+
+        for h in (0, 1):
+            @pl.when((k == plan.stripes - 1 - (1 - h) * every // 2) & ends)
+            def _():
+                product(pl.ds(rows - BLOCK + h * BLOCK // 2, BLOCK // 2))
+
     def mine(b):
         return pl.ds(pl.multiple_of(b * BLOCK + me * own_rows, own_rows), own_rows)
 
@@ -295,14 +300,14 @@
         at = pl.ds(pl.multiple_of(b * BLOCK + peer * own_rows, own_rows), own_rows)
         return pltpu.make_async_remote_copy(
             src_ref=bsend.at[at], dst_ref=brecv.at[b, k],
-            send_sem=bss.at[k], recv_sem=bsr.at[b],
+            send_sem=bss.at[k - 1], recv_sem=bsr.at[b],
             device_id={"cb": peer}, device_id_type=MESH,
         )
 
     def out_copy(b, k):
         return pltpu.make_async_remote_copy(
             src_ref=bout.at[b], dst_ref=branch_ref.at[mine(b)],
-            send_sem=oss.at[k], recv_sem=osr.at[k],
+            send_sem=oss.at[k - 1], recv_sem=osr.at[k - 1],
             device_id={"cb": (me + k) % m}, device_id_type=MESH,
         )
 
@@ -320,6 +325,56 @@
         bsend[at, :] = acc[at, :].astype(wire)
         for k in range(1, m):
             branch_copy(b, k).start()
+
+    def half_row(h, peer):
+        return pl.ds(pl.multiple_of(rows - BLOCK + h * (BLOCK // 2) + peer * half_own, half_own), half_own)
+
+    def half_copy(h, k):
+        return pltpu.make_async_remote_copy(
+            src_ref=hsend_rows.at[h, (me + k) % m], dst_ref=hrecv_rows.at[h, k],
+            send_sem=hss.at[k - 1], recv_sem=hsr.at[h],
+            device_id={"cb": (me + k) % m}, device_id_type=MESH,
+        )
+
+    def half_out(h, k):
+        return pltpu.make_async_remote_copy(
+            src_ref=hout.at[h], dst_ref=branch_ref.at[half_row(h, me)],
+            send_sem=hos.at[k - 1], recv_sem=osr.at[k - 1],
+            device_id={"cb": (me + k) % m}, device_id_type=MESH,
+        )
+
+    def keep_half(h):
+        return pltpu.make_async_copy(hout.at[h], branch_ref.at[half_row(h, me)], osl)
+
+    def send_half(h):
+        for peer in range(m):
+            hsend_rows[h, peer] = acc[half_row(h, peer), :].astype(wire)
+        for k in range(1, m):
+            half_copy(h, k).start()
+
+    def add_stat(branch, first):
+        sums = jnp.sum(branch * branch, axis=1, keepdims=True)
+        shape = (branch.shape[0], stat.shape[1])
+        lane = lax.broadcasted_iota(jnp.int32, shape, 1)
+        row = lax.broadcasted_iota(jnp.int32, shape, 0)
+        spread = jnp.sum(jnp.where(lane == first + row, sums, 0.0), axis=0, keepdims=True)
+        stat[...] = stat[...] + spread
+
+    def sum_half(h):
+        incoming = hrecv_rows.at[h, pl.ds(1, m - 1)]
+        pltpu.make_async_copy(incoming, incoming, hsr.at[h]).wait()
+        branch = acc[half_row(h, me), :]
+        for k in range(1, m):
+            branch = branch + hrecv_rows[h, k].astype(f32)
+        add_stat(branch, rows // m - own_rows + h * half_own)
+        if h:
+            for i, k in others:
+                stat_copy(i, k).start()
+            keep_stat.start()
+        hout[h] = branch.astype(bf16)
+        for k in range(1, m):
+            half_out(h, k).start()
+        keep_half(h).start()
 
     def sum_branch(b):
         branch = acc[mine(b), :]
@@ -331,22 +386,11 @@
         for k in range(1, m):
             out_copy(b, k).start()
         pltpu.make_async_copy(bout.at[b], branch_ref.at[mine(b)], osl).start()
-        sums = jnp.sum(branch * branch, axis=1, keepdims=True)
-        lanes = stat.shape[1]
-        lane = lax.broadcasted_iota(jnp.int32, (own_rows, lanes), 1)
-        row = lax.broadcasted_iota(jnp.int32, (own_rows, lanes), 0)
-        spread = jnp.sum(jnp.where(lane == b * own_rows + row, sums, 0.0), axis=0, keepdims=True)
-        stat[...] = stat[...] + spread
-
-        @pl.when(b == blocks - 1)
-        def _():
-            for i, k in others:
-                stat_copy(i, k).start()
-            keep_stat.start()
+        add_stat(branch, b * own_rows)
 
     pre_copy.wait()
 
-    def slot(s, carry):
+    def partial_slot(s):
         def take(q):
             at = part_rows(q)
             pltpu.make_async_copy(tok_hbm.at[at], tok.at[at], lsem.at[q]).wait()
@@ -369,10 +413,14 @@
 
         t = s - LAG * jnp.minimum(r, n - 1 - r)
 
-        @pl.when((t >= 0) & (t < plan.upper) & (t % plan.head == 0))
-        def _():
-            c = t // plan.head
-            pltpu.make_async_copy(w.at[c], w.at[c], wsem.at[c]).wait()
+        @pl.when((t >= 0) & (t < plan.upper) & (lax.rem(t, plan.head) == 0))
+        def _():
+            c = lax.div(t, plan.head)
+            pltpu.make_async_copy(w.at[c], w.at[c], wsem.at[lax.rem(c, 4)]).wait()
+
+            @pl.when(c + 3 < chunks)
+            def _():
+                fetch(c + 3)
 
         for order in (0, 1):
             d = (order + 1 - upper) % 2
@@ -386,9 +434,19 @@
             def _():
                 partial_step(d, i)
 
-        @pl.when((s >= 1) & (s < chunks - 1))
-        def _():
-            fetch(s + 1)
+        @pl.when(s == 0)
+        def _():
+            for copy in rest:
+                copy.start()
+            for at in (0, rows + 8):
+                scale[pl.ds(at, 8), :] = jnp.zeros((8, LANES), f32)
+                for c in range(chunks):
+                    full[c, pl.ds(at, 8), :] = jnp.zeros((8, 2 * LANES), f32)
+
+        @pl.when(s == 0)
+        def _():
+            for c in range(1, 3):
+                fetch(c)
 
         @pl.when(s == chunks)
         def _():
@@ -400,6 +458,7 @@
         def _():
             down_copy.wait()
 
+    def hidden_slot(s):
         for order in (0, 1):
             d = (order + 1 - upper) % 2
             p = place(d)
@@ -431,7 +490,8 @@
         for step in (hidden_pass, hidden_use):
             for order in (0, 1):
                 d = (order + 1 - upper) % 2
-                k, live = stripe(s - ROW_LAG * place(d))
+                held = 2 if order and step is hidden_use else 0
+                k, live = stripe(s - ROW_LAG * place(d) - held)
 
                 @pl.when(live)
                 def _():
@@ -441,19 +501,42 @@
         done = s - ROW_LAG * jnp.maximum(r, n - 1 - r)
         send_at, live = stripe(done)
 
-        @pl.when(live & (send_at % every == every - 1))
-        def _():
-            send_branch(send_at // every)
-
-        sum_at, live = stripe(done - plan.sum_after)
-
-        @pl.when(live & (sum_at % every == every - 1))
-        def _():
-            sum_branch(sum_at // every)
-
+        @pl.when(live & (lax.rem(send_at, every) == every - 1) & (send_at < plan.stripes - every))
+        def _():
+            send_branch(lax.div(send_at, every))
+
+        sum_at, sums = stripe(done - plan.sum_after)
+
+        @pl.when(sums & (lax.rem(sum_at, every) == every - 1) & (sum_at < plan.stripes - 2 * every))
+        def _():
+            sum_branch(lax.div(sum_at, every))
+
+        for h in (0, 1):
+            inner = (r > 0) & (r < n - 1)
+            last = plan.stripes - 1 - jnp.where(inner, 0, (1 - h) * every // 2)
+
+            @pl.when(live & (send_at == last))
+            def _():
+                send_half(h)
+
+    def first_slots(s, carry):
+        partial_slot(s)
         return carry
 
-    lax.fori_loop(0, plan.slots, slot, 0)
+    def mixed_slots(s, carry):
+        partial_slot(s)
+        hidden_slot(s)
+        return carry
+
+    def last_slots(s, carry):
+        hidden_slot(s)
+        return carry
+
+    lax.fori_loop(0, plan.a, first_slots, 0)
+    lax.fori_loop(plan.a, plan.tail, mixed_slots, 0)
+    lax.fori_loop(plan.tail, plan.slots, last_slots, 0)
+    sum_branch(blocks - 1)
+    sum_half(0)
 
     for d in (0, 1):
         @pl.when(place(d) < n - 1)
@@ -466,22 +549,25 @@
                 ).wait_send()
 
     for k in range(1, m):
-        peer = {"cb": (me + k) % m}
-        sent = brecv.at[:, k]
+        for buffer, sem in ((brecv.at[:, k], bss), (bout, oss)):
+            pltpu.make_async_remote_copy(
+                src_ref=buffer, dst_ref=buffer, send_sem=sem.at[k - 1], recv_sem=osr.at[k - 1],
+                device_id=somewhere(0, k), device_id_type=MESH,
+            ).wait_send()
+
+    sum_half(1)
+
+    share = branch_ref.at[pl.ds(0, rows // m)]
+    for k in range(1, m):
+        for buffer, sem in ((hrecv_rows.at[:, k], hss), (hout, hos)):
+            pltpu.make_async_remote_copy(
+                src_ref=buffer, dst_ref=buffer, send_sem=sem.at[k - 1], recv_sem=osr.at[k - 1],
+                device_id=somewhere(0, k), device_id_type=MESH,
+            ).wait_send()
         pltpu.make_async_remote_copy(
-            src_ref=sent, dst_ref=sent, send_sem=bss.at[k], recv_sem=bsr.at[0],
-            device_id=peer, device_id_type=MESH,
-        ).wait_send()
-        share = branch_ref.at[pl.ds(0, rows // m)]
-        pltpu.make_async_remote_copy(
-            src_ref=bout, dst_ref=bout, send_sem=oss.at[k], recv_sem=osr.at[k],
-            device_id=peer, device_id_type=MESH,
-        ).wait_send()
-        pltpu.make_async_remote_copy(
-            src_ref=share, dst_ref=share, send_sem=oss.at[k], recv_sem=osr.at[k],
-            device_id=peer, device_id_type=MESH,
+            src_ref=share, dst_ref=share, send_sem=oss.at[k - 1], recv_sem=osr.at[k - 1],
+            device_id=somewhere(0, k), device_id_type=MESH,
         ).wait_recv()
-    share = branch_ref.at[pl.ds(0, rows // m)]
     pltpu.make_async_copy(share, share, osl).wait()
     all_stats = stat_ref.at[pl.ds(0, len(others))]
     both = pltpu.make_async_remote_copy(
@@ -499,8 +585,9 @@
 ):
     rows, width = tok.shape
     parts = rows // PART
-    blocks = rows // BLOCK
+    blocks = rows // BLOCK - 1
     own_rows = BLOCK // m
+    half_own = own_rows // 2
     f32 = jnp.float32
     stat_copy = pltpu.make_async_copy(stat_hbm, stat, isem.at[2 * parts])
     post_copy = pltpu.make_async_copy(post_hbm, post, isem.at[2 * parts + 1])
@@ -525,6 +612,10 @@
         column = jnp.broadcast_to(inv, (LANES, rows // m)).T
         for b in range(blocks):
             scale[pl.ds(b * BLOCK + k * own_rows, own_rows), :] = column[b * own_rows:(b + 1) * own_rows]
+        for h in (0, 1):
+            first = blocks * own_rows + h * half_own
+            to = pl.ds(blocks * BLOCK + h * (BLOCK // 2) + k * half_own, half_own)
+            scale[to, :] = column[first:first + half_own]
     post_copy.wait()
     writes = []
     for q in range(parts):
@@ -581,11 +672,14 @@
             pltpu.VMEM((rows, width), wire),
             pltpu.VMEM((blocks, m, own_rows, width), wire),
             pltpu.VMEM((blocks, own_rows, width), bf16),
+            pltpu.VMEM((2, m, own_rows // 2, width), wire),
+            pltpu.VMEM((2, m, own_rows // 2, width), wire),
+            pltpu.VMEM((2, own_rows // 2, width), bf16),
             pltpu.VMEM((1, rows // m), f32),
-            dma((parts + 3,)), dma((chunks,)), dma,
+            dma((parts + 3,)), dma((4,)), dma,
             dma((2,)), dma((2, PART // FIRST)), dma((2, plan.ring)), dma((2,)),
-            dma((2,)), dma((2,)), dma((m,)), dma((blocks,)), dma((m,)), dma((m,)), dma,
-            dma, dma, dma,
+            dma((2,)), dma((2,)), dma((m - 1,)), dma((blocks,)), dma((m - 1,)), dma((m - 1,)), dma,
+            dma((m - 1,)), dma((2,)), dma((m - 1,)), dma, dma, dma,
         ],
         compiler_params=pltpu.CompilerParams(
             collective_id=0, has_side_effects=True, vmem_limit_bytes=60 * 1024 * 1024

time: 122 us -> 121 us (level)
  no operation moved by 1% of the time
where the time goes in v4:
time: 121 us
  Pallas kernels  121 us (100%)
    pallas_call x1, Pallas kernels, local(): pl.pallas_call(functools.partial(kernel, n, m, plan), out_shape=[jax.Shap...  118 us
    pallas_call x1, Pallas kernels, local(): pl.pallas_call(functools.partial(finish_kernel, n, m), out_shape=jax.Shap...  2.5 us

profile of v4, /device:TPU:0, one launch (start us, length us, event | category | flops | bytes accessed | tf_op | source)
XLA Modules:
  0.0 121.0 jit_solution(17394877138326974356)
XLA Ops:
  0.0 118.5 %shard_map.82 = (bf16[512,1024]{1,0:T(8,128)(2,1)}, f32[16,1,128]{2,1,0:T(1,128)}) custom-call(bf16[512,1024]{1,0:T(8,128)(2,1)} %bitcast.4, f32[1,1024]{1,0:T(1,128)} %bitcast.7, bf16[1024,2816]{1,0:T(8,128)(2,1)} %wg_hbm.1, bf16[1024,2816]{1,0:T(8,128)(2,1)} %wu_hbm.1, f32[3,2816]{1,0:T(4,128)} %cg_hbm.1, f32[3,2816]{1,0:T(4,128)} %cu_hbm.1, ...), custom_call_target="tpu_custom_call" | custom-call | tf_op jit(solution)/shard_map/pallas_call | solution.py:647
  118.5 2.5 %shard_map.83 = bf16[512,1024]{1,0:T(8,128)(2,1)} custom-call(bf16[512,1024]{1,0:T(8,128)(2,1)} %bitcast.5, bf16[512,1024]{1,0:T(8,128)(2,1)} %get-tuple-element.7.branch_hbm, f32[16,1,128]{2,1,0:T(1,128)} %get-tuple-element.8.stat_hbm, f32[1,1024]{1,0:T(1,128)} %bitcast.6), custom_call_target="tpu_custom_call" | custom-call | tf_op jit(solution)/shard_map/pallas_call | solution.py:688

commit v5 on v4

--- a/solution.py
+++ b/solution.py
@@ -368,8 +368,13 @@
             branch = branch + hrecv_rows[h, k].astype(f32)
         add_stat(branch, rows // m - own_rows + h * half_own)
         if h:
-            for i, k in others:
-                stat_copy(i, k).start()
+            for k in (2, 1, 3, 0) if m == 4 else range(m):
+                for j in range(n):
+                    i = (n - 1 - 2 * r + j + 2 * n) % n
+
+                    @pl.when((i != 0) | (k != 0))
+                    def _():
+                        stat_copy(i, k).start()
             keep_stat.start()
         hout[h] = branch.astype(bf16)
         for k in range(1, m):

time: 121 us -> 121 us (level)
  no operation moved by 1% of the time
where the time goes in v5:
time: 121 us
  Pallas kernels  121 us (100%)
    pallas_call x1, Pallas kernels, local(): pl.pallas_call(functools.partial(kernel, n, m, plan), out_shape=[jax.Shap...  118 us
    pallas_call x1, Pallas kernels, local(): pl.pallas_call(functools.partial(finish_kernel, n, m), out_shape=jax.Shap...  2.5 us

profile of v5, /device:TPU:0, one launch (start us, length us, event | category | flops | bytes accessed | tf_op | source)
XLA Modules:
  0.0 121.0 jit_solution(17465991061457922138)
XLA Ops:
  0.0 118.5 %shard_map.82 = (bf16[512,1024]{1,0:T(8,128)(2,1)}, f32[16,1,128]{2,1,0:T(1,128)}) custom-call(bf16[512,1024]{1,0:T(8,128)(2,1)} %bitcast.4, f32[1,1024]{1,0:T(1,128)} %bitcast.7, bf16[1024,2816]{1,0:T(8,128)(2,1)} %wg_hbm.1, bf16[1024,2816]{1,0:T(8,128)(2,1)} %wu_hbm.1, f32[3,2816]{1,0:T(4,128)} %cg_hbm.1, f32[3,2816]{1,0:T(4,128)} %cu_hbm.1, ...), custom_call_target="tpu_custom_call" | custom-call | tf_op jit(solution)/shard_map/pallas_call | solution.py:652
  118.5 2.5 %shard_map.83 = bf16[512,1024]{1,0:T(8,128)(2,1)} custom-call(bf16[512,1024]{1,0:T(8,128)(2,1)} %bitcast.5, bf16[512,1024]{1,0:T(8,128)(2,1)} %get-tuple-element.7.branch_hbm, f32[16,1,128]{2,1,0:T(1,128)} %get-tuple-element.8.stat_hbm, f32[1,1024]{1,0:T(1,128)} %bitcast.6), custom_call_target="tpu_custom_call" | custom-call | tf_op jit(solution)/shard_map/pallas_call | solution.py:693
